TPU v7x, 32 devices: a whole 2x2x4 slice. The times are simulated.
32 devices in a mesh: sp: 8 (over z, x), tp: 4 (over y, core).
Axes of the slice: x: 2, y: 2, z: 4, core: 2. Of those that a mesh axis runs over, the one named last changes fastest.
Arguments:
- block_input: bfloat16 [16384, 4096], P('sp'), may hold values from -6 to 6
- value_weight: bfloat16 [4096, 1024], P(None, 'tp'), may hold values from -0.09375 to 0.09375
- key_rows: bfloat16 [16384, 512], P('sp', 'tp'), may hold values from -1 to 1
- query_rows: bfloat16 [16384, 512], P('sp', 'tp'), may hold values from -1 to 1
- decay_pre: float32 [16, 16384], P('tp', 'sp'), may hold values from -3 to 2
- decay_log: float32 [16], P('tp'), may hold values from -16 to -2
- gate_rows: bfloat16 [16384, 1024], P('sp', 'tp'), may hold values from -6 to 6
- out_grad: bfloat16 [16384, 1024], P('sp', 'tp'), may hold values from -6 to 6
Outputs:
- key_grad: float32 [16384, 512], P('sp', 'tp')
- query_grad: float32 [16384, 512], P('sp', 'tp')
- decay_grad: float32 [16, 16384], P('tp', 'sp')
- gate_grad: float32 [16384, 1024], P('sp', 'tp')
- weight_grad: float32 [4096, 1024], P('sp', 'tp')
- row_norms: float32 [4096], P('sp')
All inputs are finite; a program needn't handle non-finite values.
Results may differ from a plain program's by a relative error of at most 0.0035.
Values sent between devices are 32-bit elements; how exact they have to be, the bound alone decides.
A program may use at most 128 MiB of HBM per device.

v0:
```python
import functools

import jax
import jax.numpy as jnp
from jax import lax
from jax.experimental import pallas as pl
from jax.experimental.pallas import tpu as pltpu
from jax.sharding import PartitionSpec as P

HEAD = 64
STATE = 64
BLK = 128

HIGH = lax.Precision.HIGHEST
BF = jnp.bfloat16
F32 = jnp.float32


def dot(a, b, ca, cb):
    return lax.dot_general(a, b, (((ca,), (cb,)), ((), ())), preferred_element_type=F32)


def load_chunk(pre_ref, gate_ref, out_ref):
    pre = pre_ref[...].astype(F32)
    gate = gate_ref[...].astype(F32)
    cot = out_ref[...].astype(F32)
    sig_pre = jax.nn.sigmoid(pre)
    sig_gate = jax.nn.sigmoid(gate)
    return pre, sig_pre, pre * sig_pre, gate, sig_gate, cot, cot * gate * sig_gate


def scales(cols_ref, heads):
    run = cols_ref[:, 0:heads]
    step = cols_ref[:, heads:2 * heads]
    end = cols_ref[BLK - 1:BLK, 0:heads]
    before = cols_ref[0:1, 2 * heads:3 * heads]
    return run, jnp.exp(run), jnp.exp(end - run) * step, jnp.exp(end), jnp.exp(before)


def states_kernel(heads, ratio, pre_ref, gate_ref, out_ref, key_ref, query_ref, cols_ref,
                  before_ref, end_ref, start_ref):
    @pl.when(pl.program_id(0) == 0)
    def _():
        end_ref[...] = jnp.zeros_like(end_ref)
        start_ref[...] = jnp.zeros_like(start_ref)

    _, _, vals, _, _, _, grads = load_chunk(pre_ref, gate_ref, out_ref)
    _, from_start, to_end, factor, before = scales(cols_ref, heads)
    before_ref[...] = end_ref[...]
    for h in range(heads):
        g = h // ratio
        sl = slice(h * HEAD, (h + 1) * HEAD)
        gs = slice(g * STATE, (g + 1) * STATE)
        contrib = dot(key_ref[:, gs], (vals[:, sl] * to_end[:, h:h + 1]).astype(BF), 0, 0)
        back = dot(query_ref[:, gs], (grads[:, sl] * from_start[:, h:h + 1]).astype(BF), 0, 0)
        end_ref[:, sl] = end_ref[:, sl] * factor[:, h:h + 1] + contrib
        start_ref[:, sl] = start_ref[:, sl] + before[:, h:h + 1] * back


def grads_kernel(heads, ratio, pre_ref, gate_ref, out_ref, key_ref, query_ref, cols_ref,
                 rows_ref, before_ref, in_ref, end_ref, outgo_ref,
                 dkey_ref, dquery_ref, dgate_ref, dval_ref, rc_ref, next_ref, dstate_ref):
    @pl.when(pl.program_id(0) == 0)
    def _():
        next_ref[...] = end_ref[...]
        dstate_ref[...] = outgo_ref[...]

    pre, sig_pre, vals, gate, sig_gate, cot, grads = load_chunk(pre_ref, gate_ref, out_ref)
    run, from_start, to_end, factor, before = scales(cols_ref, heads)
    at_q = lax.broadcasted_iota(jnp.int32, (BLK, BLK), 0)
    at_k = lax.broadcasted_iota(jnp.int32, (BLK, BLK), 1)
    lower = at_q >= at_k
    val_slope = sig_pre * (1.0 + pre * (1.0 - sig_pre))
    gate_slope = cot * sig_gate * (1.0 + gate * (1.0 - sig_gate))
    for g in range(heads // ratio):
        gs = slice(g * STATE, (g + 1) * STATE)
        key = key_ref[:, gs]
        query = query_ref[:, gs]
        scores = dot(query, key, 1, 1)
        total = None
        dkey = None
        dquery = None
        for h in range(g * ratio, (g + 1) * ratio):
            sl = slice(h * HEAD, (h + 1) * HEAD)
            spread = run[:, h:h + 1] - rows_ref[h:h + 1, :]
            decay = jnp.exp(jnp.where(lower, spread, -1e30)) * rows_ref[heads + h:heads + h + 1, :]
            weights = (scores * decay).astype(BF)
            val, grad = vals[:, sl], grads[:, sl]
            val_b, grad_b = val.astype(BF), grad.astype(BF)
            pulled = dot(grad_b, val_b, 1, 1) * decay
            total = pulled if total is None else total + pulled
            state = before_ref[:, sl] + before[:, h:h + 1] * in_ref[:, sl]
            dstate = dstate_ref[:, sl]
            state_b, dstate_b = state.astype(BF), dstate.astype(BF)
            fs, te = from_start[:, h:h + 1], to_end[:, h:h + 1]
            mixed = dot(weights, val_b, 1, 0) + dot(query, state_b, 1, 0) * fs
            dval = dot(weights, grad_b, 0, 0) + dot(key, dstate_b, 1, 0) * te
            grad_fs = (grad * fs).astype(BF)
            dq = dot(grad_fs, state_b, 1, 1)
            dk = dot((val * te).astype(BF), dstate_b, 1, 1)
            dquery = dq if dquery is None else dquery + dq
            dkey = dk if dkey is None else dkey + dk
            dgate_ref[:, sl] = mixed * gate_slope[:, sl]
            dval_ref[:, sl] = (dval * val_slope[:, sl]).astype(BF)
            cross = jnp.sum(jnp.sum(next_ref[:, sl] * dstate, axis=1, keepdims=True), axis=0,
                            keepdims=True)
            rc_ref[:, h:h + 1] = jnp.sum(grad * mixed, axis=1, keepdims=True)
            rc_ref[:, heads + h:heads + h + 1] = jnp.sum(val * dval, axis=1, keepdims=True)
            rc_ref[:, 2 * heads + h:2 * heads + h + 1] = jnp.broadcast_to(cross, (BLK, 1))
            next_ref[:, sl] = state
            dstate_ref[:, sl] = dstate * factor[:, h:h + 1] + dot(query, grad_fs, 0, 0)
        total_b = total.astype(BF)
        dquery_ref[:, gs] = dquery + dot(total_b, key, 1, 0)
        dkey_ref[:, gs] = dkey + dot(total_b, query, 0, 0)


def shards(
    block_input, value_weight, key_rows, query_rows, decay_pre, decay_log, gate_rows, out_grad
):
    heads = decay_log.shape[0]
    tokens = block_input.shape[0]
    groups = key_rows.shape[1] // STATE
    ratio = heads // groups
    wide, narrow = heads * HEAD, groups * STATE
    blocks = tokens // BLK
    projected = jnp.dot(block_input, value_weight, preferred_element_type=F32).astype(BF)

    step_sizes = jax.nn.softplus(decay_pre)
    rates = jnp.exp(decay_log)
    logs = (-rates[:, None] * step_sizes).reshape(heads, blocks, BLK)
    upto = jnp.triu(jnp.ones((BLK, BLK), F32))
    running = jnp.einsum("hbs,st->hbt", logs, upto, precision=HIGH)
    ends = running[:, :, -1]
    earlier = jnp.triu(jnp.ones((blocks, blocks), F32), 1)
    prefix = jnp.einsum("hb,bc->hc", ends, earlier, precision=HIGH)
    log_total = jnp.sum(ends, axis=1)
    rows = jnp.concatenate([running.reshape(heads, tokens), step_sizes], axis=0)
    prefix_rows = jnp.broadcast_to(prefix[:, :, None], (heads, blocks, BLK)).reshape(heads, tokens)
    cols = jnp.concatenate([rows, prefix_rows], axis=0).T

    def spec(width, rev):
        if rev:
            return pl.BlockSpec((BLK, width), lambda i: (blocks - 1 - i, 0))
        return pl.BlockSpec((BLK, width), lambda i: (i, 0))

    whole = pl.BlockSpec((STATE, wide), lambda i: (0, 0))
    state_shape = jax.ShapeDtypeStruct((STATE, wide), F32)
    params = pltpu.CompilerParams(dimension_semantics=("arbitrary",))
    before, end_state, start_grad = pl.pallas_call(
        functools.partial(states_kernel, heads, ratio),
        grid=(blocks,),
        in_specs=[spec(wide, False)] * 3 + [spec(narrow, False)] * 2 + [spec(3 * heads, False)],
        out_specs=[pl.BlockSpec((STATE, wide), lambda i: (i, 0)), whole, whole],
        out_shape=[jax.ShapeDtypeStruct((blocks * STATE, wide), F32), state_shape, state_shape],
        compiler_params=params,
        name="span_states",
    )(projected, gate_rows, out_grad, key_rows, query_rows, cols)

    lanes_total = jnp.repeat(log_total, HEAD)[None, :]
    packed = jnp.concatenate(
        [end_state, start_grad, jnp.broadcast_to(lanes_total, (8, wide))], axis=0
    )
    every = lax.all_gather(packed, "sp")
    count, index = lax.axis_size("sp"), lax.axis_index("sp")
    totals = every[:, 2 * STATE, :]
    s = jnp.arange(count)[:, None]
    j = jnp.arange(count)[None, :]
    ahead = jnp.sum(jnp.where(((s < j) & (j < index))[:, :, None], totals[None], 0.0), axis=1)
    after = jnp.sum(jnp.where(((s > j) & (j > index))[:, :, None], totals[None], 0.0), axis=1)
    ahead = jnp.where(s < index, jnp.exp(ahead), 0.0)
    after = jnp.where(s > index, jnp.exp(after), 0.0)
    incoming = jnp.sum(ahead[:, None, :] * every[:, :STATE], axis=0)
    outgoing = jnp.sum(after[:, None, :] * every[:, STATE:2 * STATE], axis=0)
    end_state = end_state + jnp.exp(lanes_total) * incoming

    key_grad, query_grad, gate_grad, value_grad, sums = pl.pallas_call(
        functools.partial(grads_kernel, heads, ratio),
        grid=(blocks,),
        in_specs=[spec(wide, True)] * 3 + [spec(narrow, True)] * 2 + [
            spec(3 * heads, True),
            pl.BlockSpec((2 * heads, BLK), lambda i: (0, blocks - 1 - i)),
            pl.BlockSpec((STATE, wide), lambda i: (blocks - 1 - i, 0)),
            whole, whole, whole,
        ],
        out_specs=[spec(narrow, True), spec(narrow, True), spec(wide, True), spec(wide, True),
                   spec(3 * heads, True)],
        out_shape=[
            jax.ShapeDtypeStruct((tokens, narrow), F32),
            jax.ShapeDtypeStruct((tokens, narrow), F32),
            jax.ShapeDtypeStruct((tokens, wide), F32),
            jax.ShapeDtypeStruct((tokens, wide), BF),
            jax.ShapeDtypeStruct((tokens, 3 * heads), F32),
        ],
        scratch_shapes=[pltpu.VMEM((STATE, wide), F32), pltpu.VMEM((STATE, wide), F32)],
        compiler_params=params,
        name="span_grads",
    )(projected, gate_rows, out_grad, key_rows, query_rows, cols, rows, before, incoming,
      end_state, outgoing)

    weight_grad = lax.psum_scatter(
        dot(block_input, value_grad, 0, 0), "sp", scatter_dimension=0, tiled=True
    )
    row_norms = lax.psum(jnp.sum(weight_grad * weight_grad, axis=1), "tp")

    sums = sums.T.reshape(3, heads, blocks, BLK)
    onward = jnp.einsum("hbs,ts->hbt", sums[0] - sums[1], upto, precision=HIGH)
    log_back = (onward + sums[2]).reshape(heads, tokens)
    size_total = sums[1].reshape(heads, tokens) / step_sizes - rates[:, None] * log_back
    decay_grad = size_total * jax.nn.sigmoid(decay_pre)
    return (key_grad, query_grad, decay_grad, gate_grad, weight_grad, row_norms)


def solution(mesh):
    in_specs = (
        P("sp", None),
        P(None, "tp"),
        P("sp", "tp"),
        P("sp", "tp"),
        P("tp", "sp"),
        P("tp"),
        P("sp", "tp"),
        P("sp", "tp"),
    )
    out_specs = (P("sp", "tp"), P("sp", "tp"), P("tp", "sp"), P("sp", "tp"), P("sp", "tp"), P("sp"))
    return jax.shard_map(shards, mesh=mesh, in_specs=in_specs, out_specs=out_specs, check_vma=False)
```

profile of v0, /device:TPU:0, one launch (start us, length us, event | category | flops | bytes accessed | tf_op | source)
XLA Modules:
  0.0 248.8 jit_solution(8409689195892492431)
XLA Ops:
  7.2 0.0 all-gather.3.cloned.1.call-start
  7.2 0.8 fusion.32
  8.0 0.8 compare_select_fusion
  8.9 0.3 fusion.4
  9.1 0.2 slice_reduce_fusion
  9.3 0.1 broadcast_in_dim.94
  9.4 0.1 broadcast_in_dim.95
  9.5 0.1 fusion.20
  9.6 0.1 broadcast_bitcast_fusion
  9.8 1.4 copy.23.cols_ref
  11.1 9.2 %convolution_convert_fusion.pre_ref = bf16[2048,256]{1,0:T(8,128)(2,1)} fusion(bf16[2048,4096]{1,0:T(8,128)(2,1)} %param.8, bf16[4096,256]{1,0:T(8,128)(2,1)S(1)} %copy-done), kind=kOutput, calls=%fused_computation.1 | convolution fusion | flops 4295491584 | bytes 19922944 | tf_op jit(solution)/shard_map/dot_general | solution.py:126
  20.4 17.1 %span_states.1 = (f32[1024,256]{1,0:T(8,128)}, f32[64,256]{1,0:T(8,128)}, f32[64,256]{1,0:T(8,128)}) custom-call(bf16[2048,256]{1,0:T(8,128)(2,1)} %convolution_convert_fusion.pre_ref, bf16[2048,256]{1,0:T(8,128)(2,1)} %gate_ref.3, bf16[2048,256]{1,0:T(8,128)(2,1)} %out_ref.3, bf16[2048,128]{1,0:T(8,128)(2,1)} %key_ref.3, bf16[2048,128]{1,0:T(8,128)(2,1)} %query_ref.3, ...), custom_call_target="tpu_custom_call" | custom-call | tf_op jit(solution)/shard_map/span_states/pallas_call | solution.py:149
  37.5 1.5 pad_maximum_fusion
  39.1 0.0 reduce-scatter.2.cloned.1.call-start
  39.2 0.6 pad_maximum_fusion.1.rows_ref
  39.8 42.9 %all-gather.3.cloned.1.call-done = f32[1088,256]{1,0:T(8,128)} async-done(((f32[136,256]{1,0:T(8,128)}), f32[1088,256]{1,0:T(8,128)}) %all-gather.3.cloned.1.call-update) | async-done | bytes 1114128 | tf_op jit(solution)/shard_map/all_gather | solution.py:163
  82.7 0.8 slice.33
  83.5 0.1 select_reduce_fusion
  83.6 0.1 exponential_select_fusion
  83.7 0.1 exponential_select_fusion.1
  83.8 1.9 fusion.1
  85.7 1.5 multiply_add_fusion.end_ref
  87.2 44.9 %span_grads.1 = (f32[2048,128]{1,0:T(8,128)}, f32[2048,128]{1,0:T(8,128)}, f32[2048,256]{1,0:T(8,128)}, bf16[2048,256]{1,0:T(8,128)(2,1)}, f32[2048,12]{1,0:T(8,128)}) custom-call(bf16[2048,256]{1,0:T(8,128)(2,1)} %convolution_convert_fusion.pre_ref, bf16[2048,256]{1,0:T(8,128)(2,1)} %gate_ref.3, bf16[2048,256]{1,0:T(8,128)(2,1)} %out_ref.3, ...), custom_call_target="tpu_custom_call" | custom-call | tf_op jit(solution)/shard_map/span_grads/pallas_call | solution.py:176
  132.1 12.6 %convolution_bitcast_fusion = f32[4096,256]{0,1:T(8,128)} fusion(bf16[2048,256]{1,0:T(8,128)(2,1)} %get-tuple-element.21, bf16[2048,4096]{1,0:T(8,128)(2,1)} %param.8), kind=kOutput, calls=%fused_computation | convolution fusion | flops 4294967296 | bytes 22020096 | tf_op jit(solution)/shard_map/dot_general | solution.py:20
  144.8 1.2 copy-done.1
  146.0 0.3 copy.24
  146.3 0.3 fusion
  146.6 0.7 divide_multiply_fusion
  147.3 84.7 %reduce-scatter.2.cloned.1.call-done = f32[512,256]{0,1:T(8,128)} async-done(((f32[4096,256]{0,1:T(8,128)}), f32[512,256]{0,1:T(8,128)}) %reduce-scatter.2.cloned.1.call-update) | async-done | bytes 524304 | tf_op jit(solution)/shard_map/reduce_scatter | solution.py:200
  232.1 1.1 multiply_reduce_fusion
  233.2 6.8 %psum.7 = f32[512]{0:T(512)} all-reduce(f32[512]{0:T(512)S(1)} %multiply_reduce_fusion), channel_id=1, replica_groups=mesh['sp'=8,'tp'=4] {'tp'}, use_global_device_ids=true, to_apply=%region_7.8 | all-reduce | flops 512 | bytes 4096 | tf_op jit(solution)/shard_map/psum | solution.py:203
  240.0 2.0 copy.25
  (19 shorter events, 0.2 us)
Async XLA Ops:
  7.2 4.0 %copy-start = (bf16[4096,256]{1,0:T(8,128)(2,1)S(1)}, bf16[4096,256]{1,0:T(8,128)(2,1)}, u32[]{:S(2)}) copy-start(bf16[4096,256]{1,0:T(8,128)(2,1)} %param.9) | copy-start | bytes 6291460
  7.2 75.5 %all-gather.3.cloned.1.call-start = ((), (), s32[]{:S(2)}) async-start(), calls=%async_computation.2 | async-start | bytes 1253376 | tf_op jit(solution)/shard_map/all_gather | solution.py:163
  39.1 193.0 %reduce-scatter.2.cloned.1.call-start = ((), (), s32[]{:S(2)}) async-start(), calls=%async_computation.1 | async-start | bytes 4718592 | tf_op jit(solution)/shard_map/reduce_scatter | solution.py:200
  85.7 1.5 copy-start.2
  144.7 1.2 copy-start.1
  144.7 1.9 copy-start.3
Sparse Core Ops, SparseCore 0:
  39.2 43.4 all-gather.2
  144.9 87.1 reduce-scatter.1
where the time goes:
time: 250 us; the launch traced here: 249 us
  waiting for transfers between devices  128 us (51%)
  Pallas kernels  62 us (25%)
  matrix products  22.5 us (9%)
  between operations  14.2 us (6%)
  other arithmetic  9.53 us (4%)
  blocking collectives  6.77 us (3%)
  local copies, waits for them, and re-layouts  6.07 us (2%)
    reduce_scatter x1, waiting for transfers between devices, shards(): lax.psum_scatter(dot(block_input, value_grad, 0, 0), 'sp', scatter_dimens...  84.7 us
    pallas_call x1, Pallas kernels, shards(): pl.pallas_call(functools.partial(grads_kernel, heads, ratio), grid=(block...  44.9 us
    all_gather x1, waiting for transfers between devices, shards(): every = lax.all_gather(packed, 'sp')  42.9 us
    pallas_call x1, Pallas kernels, shards(): pl.pallas_call(functools.partial(states_kernel, heads, ratio), grid=(bloc...  17.1 us
    dot_general x1, matrix products, dot(): lax.dot_general(a, b, (((ca,), (cb,)), ((), ())), preferred_element_type=...  12.6 us
    dot_general x1, matrix products, shards(): jnp.dot(block_input, value_weight, preferred_element_type=F32).astype(BF)  9.23 us
    psum x1, blocking collectives, shards(): row_norms = lax.psum(jnp.sum(weight_grad * weight_grad, axis=1), 'tp')  6.77 us
  transfers between devices with their start and end apart: 2, of which 2 were waited for; matrix products, arithmetic and copies ran while one was open for 1% of the time, Pallas kernels for 0%

commit v1 on v0

v1 whole, which is shorter than its diff:
```python
import functools

import jax
import jax.numpy as jnp
from jax import lax
from jax.experimental import pallas as pl
from jax.experimental.pallas import tpu as pltpu
from jax.sharding import PartitionSpec as P

HEAD = 64
STATE = 64
BLK = 128
ROWS = 8
LOADS = 8

BF = jnp.bfloat16
F32 = jnp.float32
MESH = pl.DeviceIdType.MESH


def dot(a, b, ca, cb):
    return lax.dot_general(a, b, (((ca,), (cb,)), ((), ())), preferred_element_type=F32)


def iota(shape, dim):
    return lax.broadcasted_iota(jnp.int32, shape, dim)


def sigmoid(v):
    return 1.0 / (1.0 + jnp.exp(-v))


def thirds(q):
    hi = q.astype(BF).astype(F32)
    rest = q - hi
    mid = rest.astype(BF).astype(F32)
    return jnp.concatenate([hi, mid, rest - mid], axis=0).astype(BF)


def halves(q):
    hi = q.astype(BF)
    return hi, (q - hi.astype(F32)).astype(BF)


def by_blocks(a, count, width):
    if count == 1:
        return a
    lane = iota(a.shape, 1) // width
    return jnp.concatenate([jnp.where(lane == i, a, jnp.zeros_like(a)) for i in range(count)], axis=0)


def kernel(c, x_hbm, w_hbm, key_hbm, query_hbm, pre_ref, log_ref, gate_hbm, out_hbm,
           dkey_hbm, dquery_hbm, ddecay_ref, dgate_hbm, wgrad_hbm, norm_ref,
           xv, wv, kv, qv, gv, ov, run_s, runs_s, step_s, cols_s, grads_s, gfs_s, dstates, states,
           fac_s, after_s, ahead_s, vals_s, te_s, dval_s, vslope_s, vte_s, dgate_s, dkey_s, dquery_s,
           vgt_s, part, xrecv, zbuf, rev_out, rev_in, fwd_out, fwd_in, outgo_s, income_s, wg_s, norms, fac_row,
           in_sem, x_sem, rev_ss, rev_rs, fwd_ss, fwd_rs, xs, xr, zs, zr, ns, nr, o_sem):
    heads, ratio, blocks, n, ntp, X, Z = c["heads"], c["ratio"], c["blocks"], c["n"], c["ntp"], c["X"], c["Z"]
    groups = heads // ratio
    wide, narrow, CD = heads * HEAD, groups * STATE, c["cd"]
    gw = ratio * HEAD
    PC = max(1, blocks // Z)
    PR = wide // PC
    tokens = blocks * BLK
    me, tpi = lax.axis_index("sp"), lax.axis_index("tp")
    z, x = me // X, lax.rem(me, X)

    def local(src, dst, sem):
        return pltpu.make_async_copy(src, dst, sem)

    def remote(src, dst, ssem, rsem, axis, to):
        return pltpu.make_async_remote_copy(src, dst, ssem, rsem, device_id={axis: to}, device_id_type=MESH)

    loads = [local(gate_hbm, gv, in_sem.at[0]), local(out_hbm, ov, in_sem.at[1]),
             local(query_hbm, qv, in_sem.at[2]), local(key_hbm, kv, in_sem.at[3]),
             local(w_hbm, wv, in_sem.at[4])]
    for copy in loads:
        copy.start()
    XR = tokens // LOADS

    def x_load(m):
        rows = pl.ds(pl.multiple_of(m * XR, XR), XR)
        return local(x_hbm.at[rows, :], xv.at[rows, :], x_sem.at[m])

    for m in range(LOADS):
        x_load(m).start()

    barrier = pltpu.get_barrier_semaphore()
    for d in range(1, n):
        pl.semaphore_signal(barrier, inc=1, device_id={"sp": lax.rem(me + d, n)}, device_id_type=MESH)
    for d in range(1, ntp):
        pl.semaphore_signal(barrier, inc=1, device_id={"tp": lax.rem(tpi + d, ntp)}, device_id_type=MESH)

    head_row = iota((ROWS, BLK), 0)
    rate = jnp.zeros((ROWS, BLK), F32)
    for h in range(heads):
        rate = jnp.where(head_row == h, jnp.broadcast_to(log_ref[h], (ROWS, BLK)), rate)
    rate = jnp.where(head_row < heads, jnp.exp(rate), 0.0)
    run_s[...] = jnp.zeros_like(run_s)
    for b in range(blocks):
        run_s[b * ROWS:b * ROWS + heads, :] = pre_ref[:, b * BLK:(b + 1) * BLK]
    pre_all = run_s[...]
    step_all = jnp.maximum(pre_all, 0.0) + jnp.log1p(jnp.exp(-jnp.abs(pre_all)))
    step_s[...] = step_all
    lanes = iota((blocks * ROWS, BLK), 1)
    acc = -jnp.concatenate([rate] * blocks, axis=0) * step_all
    shift = 1
    while shift < BLK:
        acc = acc + jnp.where(lanes >= shift, pltpu.roll(acc, shift, 1), 0.0)
        shift *= 2
    run_s[...] = acc
    runs_all = acc - jnp.log(step_all)
    runs_s[...] = runs_all
    for b in range(blocks):
        rows = slice(b * ROWS, (b + 1) * ROWS)
        cols_s[b * BLK:(b + 1) * BLK, :] = jnp.concatenate([acc[rows], runs_all[rows]], axis=0).T

    spread = jnp.where((iota((3 * ROWS, wide), 0) & (ROWS - 1)) == iota((3 * ROWS, wide), 1) // HEAD,
                       1.0, 0.0).astype(BF)
    own = iota((narrow, wide), 0) // STATE == iota((narrow, wide), 1) // gw
    pick = jnp.where(iota((ROWS, wide), 0) == iota((ROWS, wide), 1) // HEAD, 1.0, 0.0).astype(BF)
    at_row, at_col = iota((BLK, BLK), 0), iota((BLK, BLK), 1)

    def toks(b):
        return pl.ds(pl.multiple_of(b * BLK, BLK), BLK)

    def heads8(b):
        return pl.ds(pl.multiple_of(b * ROWS, ROWS), ROWS)

    def compact(a):
        total = a[0:STATE]
        for g in range(1, groups):
            total = total + a[g * STATE:(g + 1) * STATE]
        return total

    def widen(a):
        return jnp.where(own, jnp.concatenate([a] * groups, axis=0), 0.0)

    dstates[blocks] = jnp.zeros((narrow, wide), F32)
    for copy in loads[:3]:
        copy.wait()

    def reverse(i, decayed):
        b = blocks - 1 - i
        tk = toks(b)
        gate, cot = gv[tk, :].astype(F32), ov[tk, :].astype(F32)
        sig = sigmoid(gate)
        cs = cot * sig
        grads = cs * gate
        grads_s[tk, :] = grads
        dgate_s[tk, :] = cs * (1.0 + gate * (1.0 - sig))
        fs = dot(thirds(jnp.exp(run_s[heads8(b), :])), spread, 0, 0)
        gfs = (grads * fs).astype(BF)
        gfs_s[tk, :] = gfs
        factor = fs[BLK - 1:BLK, :]
        fac_s[b] = jnp.broadcast_to(factor, (ROWS, wide))
        after_s[b] = decayed
        back = dot(qv[tk, :], gfs, 0, 0)
        dstates[b] = dstates[b + 1] * factor + jnp.where(own, back, 0.0)
        return decayed * factor

    decayed = lax.fori_loop(0, blocks, reverse, jnp.ones((ROWS, wide), F32), unroll=2)

    rev_out[0:STATE, :] = compact(dstates[0])
    rev_out[STATE:STATE + ROWS, :] = decayed
    pl.semaphore_wait(barrier, n - 1 + ntp - 1)

    def rev_copy(d):
        return remote(rev_out, rev_in.at[d - 1], rev_ss.at[d - 1], rev_rs.at[d - 1], "sp", lax.rem(me + n - d, n))

    def fwd_copy(d):
        return remote(fwd_out, fwd_in.at[d - 1], fwd_ss.at[d - 1], fwd_rs.at[d - 1], "sp", lax.rem(me + d, n))

    for d in range(1, n):
        @pl.when(me >= d)
        def _(d=d):
            rev_copy(d).start()

    loads[4].wait()

    def project(m, carry):
        x_load(m).wait()
        rows = pl.ds(pl.multiple_of(m * XR, XR), XR)
        gv[rows, :] = jnp.dot(xv[rows, :], wv[...], preferred_element_type=F32).astype(BF)
        return carry

    lax.fori_loop(0, LOADS, project, 0)

    loads[3].wait()
    states[0] = jnp.zeros((narrow, wide), F32)

    def forward(b, before):
        tk = toks(b)
        pre = gv[tk, :].astype(F32)
        sig = sigmoid(pre)
        vals = pre * sig
        vals_s[tk, :] = vals
        vslope_s[tk, :] = sig * (1.0 + pre * (1.0 - sig))
        run, runs = run_s[heads8(b), :], runs_s[heads8(b), :]
        te = dot(thirds(jnp.exp(run[:, BLK - 1:BLK] - runs)), spread, 0, 0)
        te_s[tk, :] = te
        vte = (vals * te).astype(BF)
        vte_s[tk, :] = vte
        key, query = kv[tk, :], qv[tk, :]
        factor = fac_s[b]
        ahead_s[b] = before
        states[b + 1] = states[b] * factor[0:1] + jnp.where(own, dot(key, vte, 0, 0), 0.0)
        scores = dot(key, by_blocks(query, groups, STATE), 1, 1)
        cols = cols_s[tk, :]
        grads = grads_s[tk, :].astype(BF)
        outer = dot(key, dstates[b + 1].astype(BF), 1, 0) * te
        for g in range(groups):
            weights = []
            for h in range(g * ratio, (g + 1) * ratio):
                decay = jnp.exp(jnp.where(at_col >= at_row, run[h:h + 1, :] - cols[:, ROWS + h:ROWS + h + 1], -1e30))
                weights.append((scores[:, g * BLK:(g + 1) * BLK] * decay).astype(BF))
            gs = slice(g * gw, (g + 1) * gw)
            inner = dot(jnp.concatenate(weights, axis=1), by_blocks(grads[:, gs], ratio, HEAD), 1, 0)
            dval_s[tk, gs] = inner + outer[:, gs]
        return before * factor

    decayed = lax.fori_loop(0, blocks, forward, jnp.ones((ROWS, wide), F32), unroll=2)
    fwd_out[0:STATE, :] = compact(states[blocks])
    fwd_out[STATE:STATE + ROWS, :] = decayed
    for d in range(1, n):
        @pl.when(me + d < n)
        def _(d=d):
            fwd_copy(d).start()

    def gather(into, store, copy_of, there):
        into[...] = jnp.zeros_like(into)
        fac_row[...] = jnp.ones_like(fac_row)
        for d in range(1, n):
            @pl.when(there(d))
            def _(d=d):
                copy_of(d).wait_recv()
                into[...] += widen(store[d - 1, 0:STATE, :]) * fac_row[0:1, :]
                fac_row[...] *= store[d - 1, STATE:STATE + ROWS, :]

    gather(outgo_s, rev_in, rev_copy, lambda d: me + d < n)

    def correct(b, carry):
        tk = toks(b)
        extra = (outgo_s[...] * after_s[b][0:1]).astype(BF)
        dval = dval_s[tk, :] + dot(kv[tk, :], extra, 1, 0) * te_s[tk, :]
        dval_s[tk, :] = dval
        vgt_s[:, tk] = (dval * vslope_s[tk, :]).T.astype(BF)
        return carry

    lax.fori_loop(0, blocks, correct, 0, unroll=2)

    def chunk_of(k):
        out = jnp.int32(0)
        for i in range(Z):
            order = sorted(range(Z), key=lambda zc: -abs(zc - i))
            here = jnp.int32(0)
            for kk in range(Z):
                here = jnp.where(k == kk, order[kk], here)
            out = jnp.where(z == i, here, out)
        return out

    def x_copy(t, p):
        rows = pl.ds(pl.multiple_of(p * PR, PR), PR)
        to = z * X + lax.rem(x + 1 + t // Z, X)
        return remote(part.at[t, rows, :], xrecv.at[t, rows, :], xs.at[t * PC + p], xr.at[t * PC + p], "sp", to)

    def chunk(t, carry):
        k = lax.rem(t, Z)
        dest = chunk_of(k) * X + lax.rem(x + 1 + t // Z, X)
        for half in range(max(1, CD // 256)):
            step = min(256, CD)
            cs = pl.ds(pl.multiple_of(dest * CD + half * step, 128), step)
            part[t, :, half * step:(half + 1) * step] = jnp.dot(vgt_s[...], xv[:, cs], preferred_element_type=F32)

        @pl.when(t < (X - 1) * Z)
        def _():
            for p in range(PC):
                x_copy(t, p).start()
        return carry

    lax.fori_loop(0, X * Z, chunk, 0)

    gather(income_s, fwd_in, fwd_copy, lambda d: me >= d)

    def grads_of(b):
        tk = toks(b)
        key, query = kv[tk, :], qv[tk, :]
        grads, vals = grads_s[tk, :], vals_s[tk, :]
        grads_b, vals_b = grads.astype(BF), vals.astype(BF)
        run, runs = run_s[heads8(b), :], runs_s[heads8(b), :]
        cols = cols_s[tk, :]
        before = ahead_s[b][0:1]
        factor = fac_s[b][0:1]
        state = states[b] + before * income_s[...]
        after = states[b + 1] + (before * factor) * income_s[...]
        dstate = dstates[b + 1] + after_s[b][0:1] * outgo_s[...]
        state_b, dstate_b = state.astype(BF), dstate.astype(BF)
        keys = by_blocks(key, groups, STATE)
        scores = dot(query, keys, 1, 1)
        pulled = dot(grads_b, by_blocks(vals_b, heads, HEAD), 1, 1)
        fs = dot(thirds(jnp.exp(run)), spread, 0, 0)
        outer = dot(query, state_b, 1, 0) * fs
        totals = []
        mixed = []
        for g in range(groups):
            weights, total = [], None
            for h in range(g * ratio, (g + 1) * ratio):
                decay = jnp.exp(jnp.where(at_row >= at_col, cols[:, h:h + 1] - runs[h:h + 1, :], -1e30))
                weights.append((scores[:, g * BLK:(g + 1) * BLK] * decay).astype(BF))
                item = pulled[:, h * BLK:(h + 1) * BLK] * decay
                total = item if total is None else total + item
            totals.append(total.astype(BF))
            gs = slice(g * gw, (g + 1) * gw)
            inner = dot(jnp.concatenate(weights, axis=1), by_blocks(vals_b[:, gs], ratio, HEAD), 1, 0)
            mixed.append(inner + outer[:, gs])
        mixed = jnp.concatenate(mixed, axis=1)
        dgate_s[tk, :] = mixed * dgate_s[tk, :]
        total = jnp.concatenate(totals, axis=1)
        dquery_s[tk, :] = dot(gfs_s[tk, :], state_b, 1, 1) + dot(total, keys, 1, 0)
        across = dot(total, query, 0, 0)
        dkey = dot(vte_s[tk, :], dstate_b, 1, 1)
        mine = across[0:BLK]
        for g in range(1, groups):
            mine = jnp.where(iota((BLK, narrow), 1) // STATE == g, across[g * BLK:(g + 1) * BLK], mine)
        dkey_s[tk, :] = dkey + mine
        there = sum(dot(pick, part_, 1, 1) for part_ in halves(grads * mixed))
        here = sum(dot(pick, part_, 1, 1) for part_ in halves(vals * dval_s[tk, :]))
        cross_lanes = jnp.broadcast_to(jnp.sum(after * dstate, axis=0, keepdims=True), (ROWS, wide))
        cross = jnp.sum(jnp.where(iota((ROWS, wide), 0) == iota((ROWS, wide), 1) // HEAD, cross_lanes, 0.0),
                        axis=1, keepdims=True)
        back = there - here
        lane = iota((ROWS, BLK), 1)
        shift = 1
        while shift < BLK:
            back = back + jnp.where(lane < BLK - shift, pltpu.roll(back, BLK - shift, 1), 0.0)
            shift *= 2
        pre = pre_ref[:, tk]
        size_total = (here / step_s[heads8(b), :] - rate * (back + cross))[0:heads]
        ddecay_ref[:, tk] = size_total * sigmoid(pre)

    def z_up(k, p):
        zc = chunk_of(k)
        to = jnp.where(zc < z, z - 1, z + 1)
        slot = jnp.where((zc > z) & (zc == to), Z, zc)
        rows = pl.ds(pl.multiple_of(p * PR, PR), PR)
        return remote(part.at[(X - 1) * Z + k, rows, :], zbuf.at[slot, rows, :], zs.at[k * PC + p],
                      zr.at[slot * PC + p], "sp", lax.rem(to * X + x + n, n))

    def z_arrival(slot, p):
        rows = pl.ds(pl.multiple_of(p * PR, PR), PR)
        other = lax.rem(me + X, n)
        return remote(part.at[0, rows, :], zbuf.at[slot, rows, :], zs.at[p], zr.at[slot * PC + p], "sp", other)

    def reduce(s):
        k, p = s // PC, lax.rem(s, PC)
        zc = chunk_of(k)
        rows = pl.ds(pl.multiple_of(p * PR, PR), PR)
        mine = (X - 1) * Z + k
        total = part[mine, rows, :]
        for xi in range(X - 1):
            x_copy(xi * Z + k, p).wait_recv()
            total = total + xrecv[xi * Z + k, rows, :]
        part[mine, rows, :] = total

        @pl.when(((zc <= z) & (z < Z - 1)) | ((zc > z) & (z > 0)))
        def _():
            z_arrival(zc, p).wait_recv()
            part[mine, rows, :] += zbuf[zc, rows, :]

        @pl.when((zc == z) & (z > 0))
        def _():
            z_arrival(Z, p).wait_recv()
            part[mine, rows, :] += zbuf[Z, rows, :]

        @pl.when(zc != z)
        def _():
            z_up(k, p).start()

    outs = [local(dkey_s, dkey_hbm, o_sem.at[0]), local(dquery_s, dquery_hbm, o_sem.at[1]),
            local(dgate_s, dgate_hbm, o_sem.at[2])]
    pair = 2 if blocks % 2 == 0 else 1

    def both(s, carry):
        for i in range(pair):
            grads_of(pair * s + i)
        reduce(s)
        return carry

    def rest(s, carry):
        reduce(s)
        return carry

    early = blocks // pair
    lax.fori_loop(0, early, both, 0)
    for copy in outs:
        copy.start()
    lax.fori_loop(early, Z * PC, rest, 0)

    last = part[X * Z - 1]
    norms[tpi] = jnp.broadcast_to(jnp.sum(last * last, axis=0, keepdims=True), (ROWS, CD))

    def norm_copy(d):
        return remote(norms.at[tpi], norms.at[tpi], ns.at[d - 1], nr.at[d - 1], "tp", lax.rem(tpi + d, ntp))

    for d in range(1, ntp):
        norm_copy(d).start()
    wg_s[...] = last.T
    wcopy = local(wg_s, wgrad_hbm, o_sem.at[3])
    wcopy.start()

    for d in range(1, n):
        @pl.when(me >= d)
        def _(d=d):
            rev_copy(d).wait_send()

        @pl.when(me + d < n)
        def _(d=d):
            fwd_copy(d).wait_send()

    def sent(t, carry):
        x_copy(t // PC, lax.rem(t, PC)).wait_send()
        return carry

    lax.fori_loop(0, (X - 1) * Z * PC, sent, 0)

    def passed(t, carry):
        z_up(t // PC, lax.rem(t, PC)).wait_send()
        return carry

    lax.fori_loop(0, (Z - 1) * PC, passed, 0)
    for d in range(1, ntp):
        got = remote(norms.at[tpi], norms.at[lax.rem(tpi + ntp - d, ntp)], ns.at[d - 1], nr.at[d - 1], "tp",
                     lax.rem(tpi + d, ntp))
        got.wait()
    total = norms[0]
    for i in range(1, ntp):
        total = total + norms[i]
    norm_ref[...] = total[0:1]
    for copy in outs:
        copy.wait()
    wcopy.wait()


def shards(block_input, value_weight, key_rows, query_rows, decay_pre, decay_log, gate_rows, out_grad):
    heads = decay_log.shape[0]
    tokens, depth = block_input.shape
    groups = key_rows.shape[1] // STATE
    wide, narrow = heads * HEAD, groups * STATE
    blocks = tokens // BLK
    n, ntp = lax.axis_size("sp"), lax.axis_size("tp")
    X = max(1, ntp // 2)
    if n % X:
        X = 1
    Z = n // X
    cd = depth // n
    PC = max(1, blocks // Z)
    c = dict(heads=heads, ratio=heads // groups, blocks=blocks, n=n, ntp=ntp, X=X, Z=Z, cd=cd)
    hbm = pl.BlockSpec(memory_space=pl.ANY)
    vmem = pl.BlockSpec(memory_space=pltpu.VMEM)
    V = pltpu.VMEM
    dma = pltpu.SemaphoreType.DMA
    outs = pl.pallas_call(
        functools.partial(kernel, c),
        in_specs=[hbm, hbm, hbm, hbm, vmem, pl.BlockSpec(memory_space=pltpu.SMEM), hbm, hbm],
        out_specs=[hbm, hbm, vmem, hbm, hbm, vmem],
        out_shape=[
            jax.ShapeDtypeStruct((tokens, narrow), F32),
            jax.ShapeDtypeStruct((tokens, narrow), F32),
            jax.ShapeDtypeStruct((heads, tokens), F32),
            jax.ShapeDtypeStruct((tokens, wide), F32),
            jax.ShapeDtypeStruct((cd, wide), F32),
            jax.ShapeDtypeStruct((1, cd), F32),
        ],
        scratch_shapes=[
            V((tokens, depth), BF), V((depth, wide), BF), V((tokens, narrow), BF), V((tokens, narrow), BF),
            V((tokens, wide), BF), V((tokens, wide), BF),
            V((blocks * ROWS, BLK), F32), V((blocks * ROWS, BLK), F32), V((blocks * ROWS, BLK), F32),
            V((tokens, 2 * ROWS), F32), V((tokens, wide), F32), V((tokens, wide), BF),
            V((blocks + 1, narrow, wide), F32), V((blocks + 1, narrow, wide), F32),
            V((blocks, ROWS, wide), F32), V((blocks, ROWS, wide), F32), V((blocks, ROWS, wide), F32),
            V((tokens, wide), F32), V((tokens, wide), F32), V((tokens, wide), F32), V((tokens, wide), F32),
            V((tokens, wide), BF), V((tokens, wide), F32), V((tokens, narrow), F32), V((tokens, narrow), F32),
            V((wide, tokens), BF), V((X * Z, wide, cd), F32), V((max(1, X - 1) * Z, wide, cd), F32),
            V((Z + 1, wide, cd), F32),
            V((STATE + ROWS, wide), F32), V((n - 1, STATE + ROWS, wide), F32),
            V((STATE + ROWS, wide), F32), V((n - 1, STATE + ROWS, wide), F32),
            V((narrow, wide), F32), V((narrow, wide), F32), V((cd, wide), F32), V((ntp, ROWS, cd), F32),
            V((ROWS, wide), F32),
            dma((5,)), dma((LOADS,)), dma((n - 1,)), dma((n - 1,)), dma((n - 1,)), dma((n - 1,)),
            dma((max(1, X - 1) * Z * PC,)), dma((max(1, X - 1) * Z * PC,)),
            dma((Z * PC,)), dma(((Z + 1) * PC,)), dma((ntp - 1,)), dma((ntp - 1,)), dma((4,)),
        ],
        compiler_params=pltpu.CompilerParams(
            collective_id=0, has_side_effects=True, vmem_limit_bytes=66_000_000),
        name="mixer_back",
    )(block_input, value_weight, key_rows, query_rows, decay_pre, decay_log, gate_rows, out_grad)
    key_grad, query_grad, decay_grad, gate_grad, weight_grad, norm = outs
    return key_grad, query_grad, decay_grad, gate_grad, weight_grad, norm.reshape(cd)


def solution(mesh):
    in_specs = (
        P("sp", None),
        P(None, "tp"),
        P("sp", "tp"),
        P("sp", "tp"),
        P("tp", "sp"),
        P("tp"),
        P("sp", "tp"),
        P("sp", "tp"),
    )
    out_specs = (P("sp", "tp"), P("sp", "tp"), P("tp", "sp"), P("sp", "tp"), P("sp", "tp"), P("sp"))
    return jax.shard_map(shards, mesh=mesh, in_specs=in_specs, out_specs=out_specs, check_vma=False)
```

time: 250 us -> 88 us (0.35)
  the two profiles are of different devices: /device:TPU:0 before, /device:TPU:3 now
where the time goes in v1:
time: 88 us; the launch traced here: 87.8 us
  Pallas kernels  80.4 us (91%)
  local copies, waits for them, and re-layouts  6.76 us (8%)
    pallas_call x1, Pallas kernels, shards(): pl.pallas_call(functools.partial(kernel, c), in_specs=[hbm, hbm, hbm, hbm...  80.4 us
    unnamed x16, local copies, waits for them, and re-layouts  6.76 us

profile of v1, /device:TPU:3, one launch (start us, length us, event | category | flops | bytes accessed | tf_op | source)
XLA Modules:
  0.0 87.8 jit_solution(1346635656966447565)
XLA Ops:
  0.6 80.4 %mixer_back.1 = (f32[2048,128]{1,0:T(8,128)}, f32[2048,128]{1,0:T(8,128)}, f32[4,2048]{1,0:T(4,128)}, f32[2048,256]{1,0:T(8,128)}, f32[512,256]{1,0:T(8,128)}, /*index=5*/f32[1,512]{1,0:T(1,128)}) custom-call(bf16[2048,4096]{1,0:T(8,128)(2,1)} %x_hbm.1, bf16[4096,256]{1,0:T(8,128)(2,1)} %w_hbm.1, bf16[2048,128]{1,0:T(8,128)(2,1)} %key_hbm.1, ...), custom_call_target="tpu_custom_call" | custom-call | tf_op jit(solution)/shard_map/mixer_back/pallas_call | solution.py:462
  81.0 0.0 copy-start.1
  81.0 0.0 copy-start.3
  81.0 0.0 copy-start
  81.0 2.4 %copy.20 = f32[2048,128]{1,0:T(8,128)} copy(f32[2048,128]{1,0:T(8,128)} %get-tuple-element.24) | data formatting | bytes 2097152
  83.4 0.0 copy-done.1
  83.4 1.0 %copy.21 = f32[2048,128]{1,0:T(8,128)} copy(f32[2048,128]{1,0:T(8,128)S(1)} %copy-done.1) | data formatting | bytes 2097152
  84.4 0.0 copy-done.3
  84.4 0.6 copy.22
  85.0 0.0 copy-done
  85.0 0.0 copy-start.2
  85.0 0.0 copy-start.4
  85.0 1.3 %copy.23 = f32[2048,256]{1,0:T(8,128)} copy(f32[2048,256]{1,0:T(8,128)S(1)} %copy-done) | data formatting | bytes 4194304
  86.4 0.1 copy-done.2
  86.4 0.8 copy.24
  87.2 0.0 copy-done.4
  87.2 0.6 copy.25
Async XLA Ops:
  81.0 2.4 %copy-start.1 = (f32[2048,128]{1,0:T(8,128)S(1)}, f32[2048,128]{1,0:T(8,128)}, u32[]{:S(2)}) copy-start(f32[2048,128]{1,0:T(8,128)} %get-tuple-element.25) | copy-start | bytes 3145732
  81.0 3.4 %copy-start.3 = (f32[4,2048]{1,0:T(4,128)S(1)}, f32[4,2048]{1,0:T(4,128)}, u32[]{:S(2)}) copy-start(f32[4,2048]{1,0:T(4,128)} %get-tuple-element.26) | copy-start | bytes 98308
  81.0 4.0 %copy-start = (f32[2048,256]{1,0:T(8,128)S(1)}, f32[2048,256]{1,0:T(8,128)}, u32[]{:S(2)}) copy-start(f32[2048,256]{1,0:T(8,128)} %get-tuple-element.27) | copy-start | bytes 6291460
  85.0 1.4 %copy-start.2 = (f32[512,256]{1,0:T(8,128)S(1)}, f32[512,256]{1,0:T(8,128)}, u32[]{:S(2)}) copy-start(f32[512,256]{1,0:T(8,128)} %get-tuple-element.28) | copy-start | bytes 1572868
  85.0 2.2 %copy-start.4 = (f32[1,512]{1,0:T(1,128)S(1)}, f32[1,512]{1,0:T(1,128)}, u32[]{:S(2)}) copy-start(f32[1,512]{1,0:T(1,128)} %get-tuple-element.17) | copy-start | bytes 6148

commit v2 on v1

v2 whole, which is shorter than its diff:
```python
import functools

import jax
import jax.numpy as jnp
from jax import lax
from jax.experimental import pallas as pl
from jax.experimental.pallas import tpu as pltpu
from jax.sharding import PartitionSpec as P

HEAD = 64
STATE = 64
BLK = 128
ROWS = 8
LOADS = 8
PIECE = 32

BF = jnp.bfloat16
F32 = jnp.float32
MESH = pl.DeviceIdType.MESH


def dot(a, b, ca, cb):
    return lax.dot_general(a, b, (((ca,), (cb,)), ((), ())), preferred_element_type=F32)


def iota(shape, dim):
    return lax.broadcasted_iota(jnp.int32, shape, dim)


def sigmoid(v):
    return 1.0 / (1.0 + jnp.exp(-v))


def thirds(q):
    hi = q.astype(BF).astype(F32)
    rest = q - hi
    mid = rest.astype(BF).astype(F32)
    return jnp.concatenate([hi, mid, rest - mid], axis=0).astype(BF)


def halves(q):
    hi = q.astype(BF)
    return hi, (q - hi.astype(F32)).astype(BF)


def by_blocks(a, count, width):
    if count == 1:
        return a
    lane = iota(a.shape, 1) // width
    return jnp.concatenate([jnp.where(lane == i, a, jnp.zeros_like(a)) for i in range(count)], axis=0)


def kernel(c, x_hbm, w_hbm, key_hbm, query_hbm, pre_ref, log_ref, gate_hbm, out_hbm,
           dkey_hbm, dquery_hbm, ddecay_ref, dgate_hbm, wgrad_hbm, norm_ref,
           xv, wv, kv, qv, gv, ov, run_s, runs_s, step_s, cols_s, grads_s, gfs_s, dstates, states,
           fac_s, after_s, ahead_s, vals_s, te_s, dval_s, vslope_s, vte_s, dgate_s, dkey_s, dquery_s,
           vgt_s, part, xrecv, zbuf, zlast, xlast, row_in, col_out, col_in, outgo_s, income_s, pass_s,
           wg_s, norms,
           in_sem, x_sem, row_ss, row_rs, col_ss, col_rs, xs, xr, zs, zr, zls, zlr, xls, xlr, ns, nr, o_sem):
    heads, ratio, blocks, n, ntp, X, Z = c["heads"], c["ratio"], c["blocks"], c["n"], c["ntp"], c["X"], c["Z"]
    groups = heads // ratio
    wide, narrow, CD = heads * HEAD, groups * STATE, c["cd"]
    gw = ratio * HEAD
    PU = gw // PIECE
    NP = groups * PU
    tokens = blocks * BLK
    me, tpi = lax.axis_index("sp"), lax.axis_index("tp")
    z, x = me // X, lax.rem(me, X)

    def local(src, dst, sem):
        return pltpu.make_async_copy(src, dst, sem)

    def remote(src, dst, ssem, rsem, axis, to):
        return pltpu.make_async_remote_copy(src, dst, ssem, rsem, device_id={axis: to}, device_id_type=MESH)

    loads = [local(gate_hbm, gv, in_sem.at[0]), local(out_hbm, ov, in_sem.at[1]),
             local(query_hbm, qv, in_sem.at[2]), local(key_hbm, kv, in_sem.at[3]),
             local(w_hbm, wv, in_sem.at[4])]
    for copy in loads[:3]:
        copy.start()
    XR = tokens // LOADS

    def x_load(m):
        rows = pl.ds(pl.multiple_of(m * XR, XR), XR)
        return local(x_hbm.at[rows, :], xv.at[rows, :], x_sem.at[m])

    barrier = pltpu.get_barrier_semaphore()
    for d in range(1, n):
        pl.semaphore_signal(barrier, inc=1, device_id={"sp": lax.rem(me + d, n)}, device_id_type=MESH)
    for d in range(1, ntp):
        pl.semaphore_signal(barrier, inc=1, device_id={"tp": lax.rem(tpi + d, ntp)}, device_id_type=MESH)

    head_row = iota((ROWS, BLK), 0)
    rate = jnp.zeros((ROWS, BLK), F32)
    for h in range(heads):
        rate = jnp.where(head_row == h, jnp.broadcast_to(log_ref[h], (ROWS, BLK)), rate)
    rate = jnp.where(head_row < heads, jnp.exp(rate), 0.0)
    run_s[...] = jnp.zeros_like(run_s)
    for b in range(blocks):
        run_s[b * ROWS:b * ROWS + heads, :] = pre_ref[:, b * BLK:(b + 1) * BLK]
    pre_all = run_s[...]
    step_all = jnp.maximum(pre_all, 0.0) + jnp.log1p(jnp.exp(-jnp.abs(pre_all)))
    step_s[...] = step_all
    lanes = iota((blocks * ROWS, BLK), 1)
    acc = -jnp.concatenate([rate] * blocks, axis=0) * step_all
    shift = 1
    while shift < BLK:
        acc = acc + jnp.where(lanes >= shift, pltpu.roll(acc, shift, 1), 0.0)
        shift *= 2
    run_s[...] = acc
    runs_all = acc - jnp.log(step_all)
    runs_s[...] = runs_all
    for b in range(blocks):
        rows = slice(b * ROWS, (b + 1) * ROWS)
        cols_s[b * BLK:(b + 1) * BLK, :] = jnp.concatenate([acc[rows], runs_all[rows]], axis=0).T

    spread = jnp.where((iota((3 * ROWS, wide), 0) & (ROWS - 1)) == iota((3 * ROWS, wide), 1) // HEAD,
                       1.0, 0.0).astype(BF)
    pick = jnp.where(iota((ROWS, wide), 0) == iota((ROWS, wide), 1) // HEAD, 1.0, 0.0).astype(BF)
    at_row, at_col = iota((BLK, BLK), 0), iota((BLK, BLK), 1)

    def toks(b):
        return pl.ds(pl.multiple_of(b * BLK, BLK), BLK)

    def heads8(b):
        return pl.ds(pl.multiple_of(b * ROWS, ROWS), ROWS)

    def lanes_of(u):
        return slice(u * gw, (u + 1) * gw)

    def placed(a, u):
        rows = [a if g == u else jnp.zeros_like(a) for g in range(groups)]
        return rows[0] if groups == 1 else jnp.concatenate(rows, axis=0)

    def from_start(b, u):
        return dot(thirds(jnp.exp(run_s[heads8(b), :])), spread[:, lanes_of(u)], 0, 0)

    def to_end(b):
        run, runs = run_s[heads8(b), :], runs_s[heads8(b), :]
        return dot(thirds(jnp.exp(run[:, BLK - 1:BLK] - runs)), spread, 0, 0)

    def row_copy(i, d):
        return remote(row_in.at[i, 0], row_in.at[i, d], row_ss.at[i, d - 1], row_rs.at[i, d - 1], "sp",
                      z * X + lax.rem(x + d, X))

    def col_copy(i, d, back):
        to = lax.rem(z + (Z - d if back else d), Z) * X + x
        return remote(col_out.at[i], col_in.at[i, d - 1], col_ss.at[i, d - 1], col_rs.at[i, d - 1], "sp", to)

    def sends_to(d, back):
        return (z >= d) if back else (z + d < Z)

    def hears_from(d, back):
        return (z + d < Z) if back else (z >= d)

    def row_start(i, state, decayed):
        row_in[i, 0, 0:STATE, :] = state
        row_in[i, 0, STATE:STATE + ROWS, :] = decayed
        for d in range(1, X):
            row_copy(i, d).start()

    def row_finish(i, back):
        for d in range(1, X):
            row_copy(i, d).wait_recv()
        acc, fac = jnp.zeros((STATE, gw), F32), jnp.ones((ROWS, gw), F32)
        mine, mine_fac = acc, fac
        for xx in (reversed(range(X)) if back else range(X)):
            mine = jnp.where(x == xx, acc, mine)
            mine_fac = jnp.where(x == xx, fac, mine_fac)
            item = row_in[i, lax.rem(x - xx + X, X)]
            acc = item[0:STATE] + acc * item[STATE:STATE + 1]
            fac = fac * item[STATE:STATE + ROWS]
        pass_s[i, 0:STATE, :] = mine
        pass_s[i, STATE:STATE + ROWS, :] = mine_fac
        col_out[i, 0:STATE, :] = acc
        col_out[i, STATE:STATE + ROWS, :] = fac
        for d in range(1, Z):
            @pl.when(sends_to(d, back))
            def _(d=d):
                col_copy(i, d, back).start()

    def col_finish(i, back, into, u):
        into[u] = pass_s[i, 0:STATE, :]
        for d in range(1, Z):
            @pl.when(hears_from(d, back))
            def _(d=d):
                col_copy(i, d, back).wait_recv()
                into[u] += col_in[i, d - 1, 0:STATE, :] * pass_s[i, STATE:STATE + 1, :]
                pass_s[i, STATE:STATE + ROWS, :] *= col_in[i, d - 1, STATE:STATE + ROWS, :]

    for copy in loads[:3]:
        copy.wait()
    for copy in loads[3:]:
        copy.start()
    for m in range(LOADS):
        x_load(m).start()

    def reverse(u):
        gs = lanes_of(u)
        dstates[u, blocks] = jnp.zeros((STATE, gw), F32)

        def body(i, decayed):
            b = blocks - 1 - i
            tk = toks(b)
            gate, cot = gv[tk, gs].astype(F32), ov[tk, gs].astype(F32)
            sig = sigmoid(gate)
            cs = cot * sig
            grads = cs * gate
            grads_s[tk, gs] = grads
            dgate_s[tk, gs] = cs * (1.0 + gate * (1.0 - sig))
            fs = from_start(b, u)
            gfs = (grads * fs).astype(BF)
            gfs_s[tk, gs] = gfs
            factor = fs[BLK - 1:BLK, :]
            fac_s[b, :, gs] = jnp.broadcast_to(factor, (ROWS, gw))
            after_s[b, :, gs] = decayed
            back = dot(qv[tk, :], gfs, 0, 0)[u * STATE:(u + 1) * STATE]
            dstates[u, b] = dstates[u, b + 1] * factor + back
            return decayed * factor

        return lax.fori_loop(0, blocks, body, jnp.ones((ROWS, gw), F32), unroll=4)

    def inner_grads(u, b):
        gs = lanes_of(u)
        tk = toks(b)
        run = run_s[heads8(b), :]
        key, query = kv[tk, :], qv[tk, :]
        if u == 0:
            te_all = to_end(b)
            te_s[tk, :] = te_all
            te = te_all[:, gs]
        else:
            te = te_s[tk, gs]
        mine = iota((BLK, narrow), 1) // STATE == u
        scores = dot(key, jnp.where(mine, query, jnp.zeros_like(query)), 1, 1)
        cols = cols_s[tk, :]
        outer = dot(key, placed(dstates[u, b + 1].astype(BF), u), 1, 0) * te
        weights = []
        for h in range(u * ratio, (u + 1) * ratio):
            decay = jnp.exp(jnp.where(at_col >= at_row, run[h:h + 1, :] - cols[:, ROWS + h:ROWS + h + 1], -1e30))
            weights.append((scores * decay).astype(BF))
        spread_grads = by_blocks(grads_s[tk, gs].astype(BF), ratio, HEAD)
        dval_s[tk, gs] = dot(jnp.concatenate(weights, axis=1), spread_grads, 1, 0) + outer

    def forward():
        for u in range(groups):
            states[u, 0] = jnp.zeros((STATE, gw), F32)

        def body(b, before):
            tk = toks(b)
            vte = (vals_s[tk, :] * te_s[tk, :]).astype(BF)
            vte_s[tk, :] = vte
            factor = fac_s[b]
            ahead_s[b] = before
            add = dot(kv[tk, :], vte, 0, 0)
            for u in range(groups):
                gs = lanes_of(u)
                states[u, b + 1] = states[u, b] * factor[0:1, gs] + add[u * STATE:(u + 1) * STATE, gs]
            return before * factor

        return lax.fori_loop(0, blocks, body, jnp.ones((ROWS, wide), F32), unroll=4)

    def correct(u):
        gs = lanes_of(u)

        def body(b, carry):
            tk = toks(b)
            extra = (outgo_s[u] * after_s[b, 0:1, gs]).astype(BF)
            dval = dval_s[tk, gs] + dot(kv[tk, :], placed(extra, u), 1, 0) * te_s[tk, gs]
            dval_s[tk, gs] = dval
            vgt_s[gs, tk] = (dval * vslope_s[tk, gs]).T.astype(BF)
            return carry

        lax.fori_loop(0, blocks, body, 0, unroll=4)

    def chunk_of(k):
        out = jnp.int32(0)
        for i in range(Z):
            order = sorted(range(Z), key=lambda zc: -abs(zc - i))
            here = jnp.int32(0)
            for kk in range(Z):
                here = jnp.where(k == kk, order[kk], here)
            out = jnp.where(z == i, here, out)
        return out

    def piece_rows(q):
        return pl.ds(pl.multiple_of(q * PIECE, PIECE), PIECE)

    def x_copy(t, q):
        to = z * X + lax.rem(x + 1 + t // Z, X)
        return remote(part.at[t, piece_rows(q), :], xrecv.at[t, piece_rows(q), :], xs.at[t * NP + q],
                      xr.at[t * NP + q], "sp", to)

    def z_next(zc):
        to = jnp.where(zc < z, z - 1, z + 1)
        slot = jnp.where((zc > z) & (zc == to), Z, zc)
        return lax.rem(to * X + x + n, n), slot

    def z_copy(k, q):
        to, slot = z_next(chunk_of(k))
        return remote(part.at[(X - 1) * Z + k, piece_rows(q), :], zbuf.at[slot, piece_rows(q), :],
                      zs.at[k * NP + q], zr.at[slot * NP + q], "sp", to)

    def z_arrival(slot, q):
        return remote(part.at[0, piece_rows(q), :], zbuf.at[slot, piece_rows(q), :], zs.at[q],
                      zr.at[slot * NP + q], "sp", lax.rem(me + X, n))

    def zl_copy(t):
        to, slot = z_next(chunk_of(lax.rem(t, Z)))
        at = (t // Z) * (Z + 1) + slot
        return remote(part.at[t, 0:PIECE, :], zlast.at[at], zls.at[t], zlr.at[at], "sp", to)

    def zl_arrival(at):
        return remote(part.at[0, 0:PIECE, :], zlast.at[at], zls.at[0], zlr.at[at], "sp", lax.rem(me + X, n))

    def xl_copy(xi):
        k = Z - 1
        return remote(part.at[xi * Z + k, 0:PIECE, :], xlast.at[xi], xls.at[xi], xlr.at[xi], "sp",
                      z * X + lax.rem(x + 1 + xi, X))

    def upstream(zc):
        return ((zc <= z) & (z < Z - 1)) | ((zc > z) & (z > 0))

    def chunks(u, low, high, beside):
        def body(t, carry):
            beside(t)
            k = lax.rem(t, Z)
            zc = chunk_of(k)
            dest = zc * X + lax.rem(x + 1 + t // Z, X)
            step = min(256, CD)
            for half in range(CD // step):
                cs = pl.ds(pl.multiple_of(dest * CD + half * step, 128), step)
                part[t, lanes_of(u), half * step:(half + 1) * step] = jnp.dot(
                    vgt_s[lanes_of(u), :], xv[:, cs], preferred_element_type=F32)

            @pl.when(t < (X - 1) * Z)
            def _():
                for q in range(u * PU, (u + 1) * PU):
                    if q > 0:
                        x_copy(t, q).start()

            if u == 0:
                @pl.when((zc != z) & jnp.logical_not(upstream(zc)))
                def _():
                    zl_copy(t).start()
            return carry

        lax.fori_loop(low, high, body, 0)

    def last_rows(i, carry):
        k = i // X
        xi = lax.rem(i, X)
        t = xi * Z + k
        zc = chunk_of(k)
        base = xi * (Z + 1)

        @pl.when(upstream(zc))
        def _():
            zl_arrival(base + zc).wait_recv()
            part[t, 0:PIECE, :] += zlast[base + zc]

        @pl.when((zc == z) & (z > 0))
        def _():
            zl_arrival(base + Z).wait_recv()
            part[t, 0:PIECE, :] += zlast[base + Z]

        @pl.when((zc != z) & upstream(zc))
        def _():
            zl_copy(t).start()

        @pl.when((zc == z) & (xi < X - 1))
        def _():
            xl_copy(xi).start()
        return carry

    def grads_of(b):
        tk = toks(b)
        key, query = kv[tk, :], qv[tk, :]
        grads, vals = grads_s[tk, :], vals_s[tk, :]
        grads_b, vals_b = grads.astype(BF), vals.astype(BF)
        run, runs = run_s[heads8(b), :], runs_s[heads8(b), :]
        cols = cols_s[tk, :]
        state, dstate, cross_lanes = [], [], []
        for u in range(groups):
            gs = lanes_of(u)
            before, factor = ahead_s[b, 0:1, gs], fac_s[b, 0:1, gs]
            state.append(placed((states[u, b] + before * income_s[u]).astype(BF), u))
            after = states[u, b + 1] + (before * factor) * income_s[u]
            down = dstates[u, b + 1] + after_s[b, 0:1, gs] * outgo_s[u]
            dstate.append(placed(down.astype(BF), u))
            cross_lanes.append(jnp.sum(after * down, axis=0, keepdims=True))
        join = (lambda v: v[0]) if groups == 1 else (lambda v: jnp.concatenate(v, axis=1))
        state_b, dstate_b = join(state), join(dstate)
        keys = by_blocks(key, groups, STATE)
        scores = dot(query, keys, 1, 1)
        pulled = dot(grads_b, by_blocks(vals_b, heads, HEAD), 1, 1)
        fs = dot(thirds(jnp.exp(run)), spread, 0, 0)
        outer = dot(query, state_b, 1, 0) * fs
        totals = []
        mixed = []
        for g in range(groups):
            weights, total = [], None
            for h in range(g * ratio, (g + 1) * ratio):
                decay = jnp.exp(jnp.where(at_row >= at_col, cols[:, h:h + 1] - runs[h:h + 1, :], -1e30))
                weights.append((scores[:, g * BLK:(g + 1) * BLK] * decay).astype(BF))
                item = pulled[:, h * BLK:(h + 1) * BLK] * decay
                total = item if total is None else total + item
            totals.append(total.astype(BF))
            gs = lanes_of(g)
            inner = dot(jnp.concatenate(weights, axis=1), by_blocks(vals_b[:, gs], ratio, HEAD), 1, 0)
            mixed.append(inner + outer[:, gs])
        mixed = join(mixed)
        dgate_s[tk, :] = mixed * dgate_s[tk, :]
        total = join(totals)
        dquery_s[tk, :] = dot(gfs_s[tk, :], state_b, 1, 1) + dot(total, keys, 1, 0)
        across = dot(total, query, 0, 0)
        dkey = dot(vte_s[tk, :], dstate_b, 1, 1)
        mine = across[0:BLK]
        for g in range(1, groups):
            mine = jnp.where(iota((BLK, narrow), 1) // STATE == g, across[g * BLK:(g + 1) * BLK], mine)
        dkey_s[tk, :] = dkey + mine
        there = sum(dot(pick, part_, 1, 1) for part_ in halves(grads * mixed))
        here = sum(dot(pick, part_, 1, 1) for part_ in halves(vals * dval_s[tk, :]))
        cross = jnp.sum(jnp.where(iota((ROWS, wide), 0) == iota((ROWS, wide), 1) // HEAD, join(cross_lanes), 0.0),
                        axis=1, keepdims=True)
        back = there - here
        lane = iota((ROWS, BLK), 1)
        shift = 1
        while shift < BLK:
            back = back + jnp.where(lane < BLK - shift, pltpu.roll(back, BLK - shift, 1), 0.0)
            shift *= 2
        pre = pre_ref[:, tk]
        size_total = (here / step_s[heads8(b), :] - rate * (back + cross))[0:heads]
        ddecay_ref[:, tk] = size_total * sigmoid(pre)

    pass0, pass1 = (Z - 1) * (PU - 1), (Z - 1) * PU * (groups - 1)

    def reduce(s):
        less = max(1, PU - 1)
        r = jnp.clip(s - pass0, 0, max(0, pass1 - 1))
        k = jnp.where(s < pass0, s // less, lax.rem(r // PU, max(1, Z - 1)))
        q = jnp.where(s < pass0, 1 + lax.rem(s, less), (1 + r // (PU * max(1, Z - 1))) * PU + lax.rem(r, PU))
        k = jnp.where(s < pass0 + pass1, k, Z - 1)
        q = jnp.where(s < pass0 + pass1, q, 1 + jnp.maximum(s - pass0 - pass1, 0))
        zc = chunk_of(k)
        rows = piece_rows(q)
        mine = (X - 1) * Z + k
        total = part[mine, rows, :]
        for xi in range(X - 1):
            x_copy(xi * Z + k, q).wait_recv()
            total = total + xrecv[xi * Z + k, rows, :]
        part[mine, rows, :] = total

        @pl.when(upstream(zc))
        def _():
            z_arrival(zc, q).wait_recv()
            part[mine, rows, :] += zbuf[zc, rows, :]

        @pl.when((zc == z) & (z > 0))
        def _():
            z_arrival(Z, q).wait_recv()
            part[mine, rows, :] += zbuf[Z, rows, :]

        @pl.when(zc != z)
        def _():
            z_copy(k, q).start()

    REV, FWD = 0, groups
    for u in range(groups):
        decayed = reverse(u)
        if u == 0:
            pl.semaphore_wait(barrier, n - 1 + ntp - 1)
        row_start(REV + u, dstates[u, 0], decayed)
    row_finish(REV, True)
    for copy in loads[3:]:
        copy.wait()
    per = blocks // LOADS

    def project(m, carry):
        x_load(m).wait()
        rows = pl.ds(pl.multiple_of(m * XR, XR), XR)
        pre = jnp.dot(xv[rows, :], wv[...], preferred_element_type=F32).astype(BF).astype(F32)
        sig = sigmoid(pre)
        vals_s[rows, :] = pre * sig
        vslope_s[rows, :] = sig * (1.0 + pre * (1.0 - sig))
        for i in range(per):
            inner_grads(0, m * per + i)
        return carry

    half = LOADS // 2
    lax.fori_loop(0, half, project, 0)
    for u in range(1, groups):
        row_finish(REV + u, True)
    lax.fori_loop(half, LOADS, project, 0)
    decayed = forward()
    for u in range(groups):
        row_start(FWD + u, states[u, blocks], decayed[:, lanes_of(u)])
    col_finish(REV, True, outgo_s, 0)
    correct(0)
    steps = Z * (NP - 1)
    early = min(2 * (Z - 1), X * Z, (Z - 1) * (PU - 1)) if groups > 1 else 0
    at_end = (z == 0) | (z == Z - 1)

    def quiet(t):
        pass

    def early_step(t):
        @pl.when(at_end & (t < early))
        def _():
            reduce(t)

    chunks(0, 0, Z, quiet)
    for u in range(groups):
        row_finish(FWD + u, False)
    chunks(0, Z, X * Z, quiet)
    for u in range(1, groups):
        def inner(b, carry, u=u):
            inner_grads(u, b)
            return carry

        lax.fori_loop(0, blocks, inner, 0, unroll=4)
        col_finish(REV + u, True, outgo_s, u)
        correct(u)
        chunks(u, 0, X * Z, early_step if u == 1 else quiet)

    def alone(s, carry):
        @pl.when(jnp.logical_not(at_end & (s < early)))
        def _():
            reduce(s)
        return carry

    near = (Z - 1) * X
    lax.fori_loop(0, near, last_rows, 0)
    lax.fori_loop(0, early, alone, 0)
    for u in range(groups):
        col_finish(FWD + u, False, income_s, u)

    def both(i, carry):
        for r in range(2):
            @pl.when(early + 2 * i + r < steps)
            def _(r=r):
                reduce(early + 2 * i + r)

        @pl.when(i == blocks // 4)
        def _():
            lax.fori_loop(near, Z * X, last_rows, 0)

        for r in range(2):
            grads_of(2 * i + r)
        return carry

    lax.fori_loop(0, blocks // 2, both, 0)
    outs = [local(dkey_s, dkey_hbm, o_sem.at[0]), local(dquery_s, dquery_hbm, o_sem.at[1]),
            local(dgate_s, dgate_hbm, o_sem.at[2])]
    for copy in outs:
        copy.start()
    if early + blocks < steps:
        lax.fori_loop(early + blocks, steps, alone, 0)

    own = X * Z - 1
    for xi in range(X - 1):
        xl_copy(xi).wait_recv()
        part[own, 0:PIECE, :] += xlast[xi]
    last = part[own]
    norms[tpi] = jnp.broadcast_to(jnp.sum(last * last, axis=0, keepdims=True), (ROWS, CD))

    def norm_copy(d):
        return remote(norms.at[tpi], norms.at[tpi], ns.at[d - 1], nr.at[d - 1], "tp", lax.rem(tpi + d, ntp))

    for d in range(1, ntp):
        norm_copy(d).start()
    wg_s[...] = last.T
    wcopy = local(wg_s, wgrad_hbm, o_sem.at[3])
    wcopy.start()

    for i in range(2 * groups):
        back = i < groups
        for d in range(1, X):
            row_copy(i, d).wait_send()
        for d in range(1, Z):
            @pl.when(sends_to(d, back))
            def _(i=i, d=d, back=back):
                col_copy(i, d, back).wait_send()

    def sent(t, carry):
        x_copy(t // (NP - 1), 1 + lax.rem(t, NP - 1)).wait_send()
        return carry

    def passed(t, carry):
        z_copy(t // (NP - 1), 1 + lax.rem(t, NP - 1)).wait_send()
        return carry

    def passed_last(i, carry):
        zl_copy((i // (Z - 1)) * Z + lax.rem(i, Z - 1)).wait_send()
        return carry

    lax.fori_loop(0, (X - 1) * Z * (NP - 1), sent, 0)
    lax.fori_loop(0, (Z - 1) * (NP - 1), passed, 0)
    lax.fori_loop(0, X * (Z - 1), passed_last, 0)
    for xi in range(X - 1):
        xl_copy(xi).wait_send()
    for d in range(1, ntp):
        got = remote(norms.at[tpi], norms.at[lax.rem(tpi + ntp - d, ntp)], ns.at[d - 1], nr.at[d - 1], "tp",
                     lax.rem(tpi + d, ntp))
        got.wait()
    total = norms[0]
    for i in range(1, ntp):
        total = total + norms[i]
    norm_ref[...] = total[0:1]
    for copy in outs:
        copy.wait()
    wcopy.wait()


def shards(block_input, value_weight, key_rows, query_rows, decay_pre, decay_log, gate_rows, out_grad):
    heads = decay_log.shape[0]
    tokens, depth = block_input.shape
    groups = key_rows.shape[1] // STATE
    wide, narrow = heads * HEAD, groups * STATE
    blocks = tokens // BLK
    n, ntp = lax.axis_size("sp"), lax.axis_size("tp")
    X = max(1, ntp // 2)
    if n % X:
        X = 1
    Z = n // X
    cd = depth // n
    gw = heads // groups * HEAD
    NP = wide // PIECE
    XO = max(1, X - 1)
    c = dict(heads=heads, ratio=heads // groups, blocks=blocks, n=n, ntp=ntp, X=X, Z=Z, cd=cd)
    hbm = pl.BlockSpec(memory_space=pl.ANY)
    vmem = pl.BlockSpec(memory_space=pltpu.VMEM)
    V = pltpu.VMEM
    dma = pltpu.SemaphoreType.DMA
    outs = pl.pallas_call(
        functools.partial(kernel, c),
        in_specs=[hbm, hbm, hbm, hbm, vmem, pl.BlockSpec(memory_space=pltpu.SMEM), hbm, hbm],
        out_specs=[hbm, hbm, vmem, hbm, hbm, vmem],
        out_shape=[
            jax.ShapeDtypeStruct((tokens, narrow), F32),
            jax.ShapeDtypeStruct((tokens, narrow), F32),
            jax.ShapeDtypeStruct((heads, tokens), F32),
            jax.ShapeDtypeStruct((tokens, wide), F32),
            jax.ShapeDtypeStruct((cd, wide), F32),
            jax.ShapeDtypeStruct((1, cd), F32),
        ],
        scratch_shapes=[
            V((tokens, depth), BF), V((depth, wide), BF), V((tokens, narrow), BF), V((tokens, narrow), BF),
            V((tokens, wide), BF), V((tokens, wide), BF),
            V((blocks * ROWS, BLK), F32), V((blocks * ROWS, BLK), F32), V((blocks * ROWS, BLK), F32),
            V((tokens, 2 * ROWS), F32), V((tokens, wide), F32), V((tokens, wide), BF),
            V((groups, blocks + 1, STATE, gw), F32), V((groups, blocks + 1, STATE, gw), F32),
            V((blocks, ROWS, wide), F32), V((blocks, ROWS, wide), F32), V((blocks, ROWS, wide), F32),
            V((tokens, wide), F32), V((tokens, wide), F32), V((tokens, wide), F32), V((tokens, wide), F32),
            V((tokens, wide), BF), V((tokens, wide), F32), V((tokens, narrow), F32), V((tokens, narrow), F32),
            V((wide, tokens), BF), V((X * Z, wide, cd), F32), V((XO * Z, wide, cd), F32),
            V((Z + 1, wide, cd), F32), V((X * (Z + 1), PIECE, cd), F32), V((XO, PIECE, cd), F32),
            V((2 * groups, X, STATE + ROWS, gw), F32), V((2 * groups, STATE + ROWS, gw), F32),
            V((2 * groups, Z - 1, STATE + ROWS, gw), F32),
            V((groups, STATE, gw), F32), V((groups, STATE, gw), F32), V((2 * groups, STATE + ROWS, gw), F32),
            V((cd, wide), F32), V((ntp, ROWS, cd), F32),
            dma((5,)), dma((LOADS,)),
            dma((2 * groups, XO)), dma((2 * groups, XO)), dma((2 * groups, Z - 1)), dma((2 * groups, Z - 1)),
            dma((XO * Z * NP,)), dma((XO * Z * NP,)), dma((Z * NP,)), dma(((Z + 1) * NP,)),
            dma((X * Z,)), dma((X * (Z + 1),)), dma((XO,)), dma((XO,)),
            dma((ntp - 1,)), dma((ntp - 1,)), dma((4,)),
        ],
        compiler_params=pltpu.CompilerParams(
            collective_id=0, has_side_effects=True, vmem_limit_bytes=66_000_000),
        name="mixer_back",
    )(block_input, value_weight, key_rows, query_rows, decay_pre, decay_log, gate_rows, out_grad)
    key_grad, query_grad, decay_grad, gate_grad, weight_grad, norm = outs
    return key_grad, query_grad, decay_grad, gate_grad, weight_grad, norm.reshape(cd)


def solution(mesh):
    in_specs = (
        P("sp", None),
        P(None, "tp"),
        P("sp", "tp"),
        P("sp", "tp"),
        P("tp", "sp"),
        P("tp"),
        P("sp", "tp"),
        P("sp", "tp"),
    )
    out_specs = (P("sp", "tp"), P("sp", "tp"), P("tp", "sp"), P("sp", "tp"), P("sp", "tp"), P("sp"))
    return jax.shard_map(shards, mesh=mesh, in_specs=in_specs, out_specs=out_specs, check_vma=False)
```

time: 88 us -> 77.5 us (0.88)
  the two profiles are of different devices: /device:TPU:3 before, /device:TPU:0 now
where the time goes in v2:
time: 77.5 us; the launch traced here: 77.2 us
  Pallas kernels  69.8 us (90%)
  local copies, waits for them, and re-layouts  6.76 us (9%)
    pallas_call x1, Pallas kernels, shards(): pl.pallas_call(functools.partial(kernel, c), in_specs=[hbm, hbm, hbm, hbm...  69.8 us
    unnamed x16, local copies, waits for them, and re-layouts  6.76 us

profile of v2, /device:TPU:0, one launch (start us, length us, event | category | flops | bytes accessed | tf_op | source)
XLA Modules:
  0.0 77.2 jit_solution(9652735482639588331)
XLA Ops:
  0.6 69.8 %mixer_back.1 = (f32[2048,128]{1,0:T(8,128)}, f32[2048,128]{1,0:T(8,128)}, f32[4,2048]{1,0:T(4,128)}, f32[2048,256]{1,0:T(8,128)}, f32[512,256]{1,0:T(8,128)}, /*index=5*/f32[1,512]{1,0:T(1,128)}) custom-call(bf16[2048,4096]{1,0:T(8,128)(2,1)} %x_hbm.1, bf16[4096,256]{1,0:T(8,128)(2,1)} %w_hbm.1, bf16[2048,128]{1,0:T(8,128)(2,1)} %key_hbm.1, ...), custom_call_target="tpu_custom_call" | custom-call | tf_op jit(solution)/shard_map/mixer_back/pallas_call | solution.py:635
  70.4 0.0 copy-start.1
  70.4 0.0 copy-start.3
  70.5 0.0 copy-start
  70.5 2.4 %copy.20 = f32[2048,128]{1,0:T(8,128)} copy(f32[2048,128]{1,0:T(8,128)} %get-tuple-element.24) | data formatting | bytes 2097152
  72.9 0.0 copy-done.1
  72.9 1.0 %copy.21 = f32[2048,128]{1,0:T(8,128)} copy(f32[2048,128]{1,0:T(8,128)S(1)} %copy-done.1) | data formatting | bytes 2097152
  73.8 0.0 copy-done.3
  73.8 0.6 copy.22
  74.5 0.0 copy-done
  74.5 0.0 copy-start.2
  74.5 0.0 copy-start.4
  74.5 1.3 %copy.23 = f32[2048,256]{1,0:T(8,128)} copy(f32[2048,256]{1,0:T(8,128)S(1)} %copy-done) | data formatting | bytes 4194304
  75.8 0.1 copy-done.2
  75.8 0.8 %copy.24 = f32[512,256]{1,0:T(8,128)} copy(f32[512,256]{1,0:T(8,128)S(1)} %copy-done.2) | data formatting | bytes 1048576
  76.6 0.0 copy-done.4
  76.6 0.6 copy.25
Async XLA Ops:
  70.4 2.4 %copy-start.1 = (f32[2048,128]{1,0:T(8,128)S(1)}, f32[2048,128]{1,0:T(8,128)}, u32[]{:S(2)}) copy-start(f32[2048,128]{1,0:T(8,128)} %get-tuple-element.25) | copy-start | bytes 3145732
  70.4 3.4 %copy-start.3 = (f32[4,2048]{1,0:T(4,128)S(1)}, f32[4,2048]{1,0:T(4,128)}, u32[]{:S(2)}) copy-start(f32[4,2048]{1,0:T(4,128)} %get-tuple-element.26) | copy-start | bytes 98308
  70.5 4.0 %copy-start = (f32[2048,256]{1,0:T(8,128)S(1)}, f32[2048,256]{1,0:T(8,128)}, u32[]{:S(2)}) copy-start(f32[2048,256]{1,0:T(8,128)} %get-tuple-element.27) | copy-start | bytes 6291460
  74.5 1.4 %copy-start.2 = (f32[512,256]{1,0:T(8,128)S(1)}, f32[512,256]{1,0:T(8,128)}, u32[]{:S(2)}) copy-start(f32[512,256]{1,0:T(8,128)} %get-tuple-element.28) | copy-start | bytes 1572868
  74.5 2.2 %copy-start.4 = (f32[1,512]{1,0:T(1,128)S(1)}, f32[1,512]{1,0:T(1,128)}, u32[]{:S(2)}) copy-start(f32[1,512]{1,0:T(1,128)} %get-tuple-element.17) | copy-start | bytes 6148

commit v3 on v2

--- a/solution.py
+++ b/solution.py
@@ -51,11 +51,11 @@
 
 
 def kernel(c, x_hbm, w_hbm, key_hbm, query_hbm, pre_ref, log_ref, gate_hbm, out_hbm,
-           dkey_hbm, dquery_hbm, ddecay_ref, dgate_hbm, wgrad_hbm, norm_ref,
+           dkey_hbm, dquery_hbm, ddecay_hbm, dgate_hbm, wgrad_hbm, norm_hbm,
            xv, wv, kv, qv, gv, ov, run_s, runs_s, step_s, cols_s, grads_s, gfs_s, dstates, states,
            fac_s, after_s, ahead_s, vals_s, te_s, dval_s, vslope_s, vte_s, dgate_s, dkey_s, dquery_s,
            vgt_s, part, xrecv, zbuf, zlast, xlast, row_in, col_out, col_in, outgo_s, income_s, pass_s,
-           wg_s, norms,
+           wg_s, norms, ddecay_s, norm_s,
            in_sem, x_sem, row_ss, row_rs, col_ss, col_rs, xs, xr, zs, zr, zls, zlr, xls, xlr, ns, nr, o_sem):
     heads, ratio, blocks, n, ntp, X, Z = c["heads"], c["ratio"], c["blocks"], c["n"], c["ntp"], c["X"], c["Z"]
     groups = heads // ratio
@@ -192,8 +192,6 @@
         copy.wait()
     for copy in loads[3:]:
         copy.start()
-    for m in range(LOADS):
-        x_load(m).start()
 
     def reverse(u):
         gs = lanes_of(u)
@@ -431,7 +429,7 @@
             shift *= 2
         pre = pre_ref[:, tk]
         size_total = (here / step_s[heads8(b), :] - rate * (back + cross))[0:heads]
-        ddecay_ref[:, tk] = size_total * sigmoid(pre)
+        ddecay_s[:, tk] = size_total * sigmoid(pre)
 
     pass0, pass1 = (Z - 1) * (PU - 1), (Z - 1) * PU * (groups - 1)
 
@@ -466,15 +464,26 @@
             z_copy(k, q).start()
 
     REV, FWD = 0, groups
+    decays = []
     for u in range(groups):
-        decayed = reverse(u)
+        decays.append(reverse(u))
         if u == 0:
-            pl.semaphore_wait(barrier, n - 1 + ntp - 1)
-        row_start(REV + u, dstates[u, 0], decayed)
-    row_finish(REV, True)
-    for copy in loads[3:]:
-        copy.wait()
-    per = blocks // LOADS
+            for m in range(LOADS):
+                x_load(m).start()
+    loads[3].wait()
+
+    def inner(u):
+        def body(b, carry):
+            inner_grads(u, b)
+            return carry
+        return body
+
+    lead = max(0, blocks - LOADS)
+    lax.fori_loop(0, lead, inner(0), 0, unroll=4)
+    pl.semaphore_wait(barrier, n - 1 + ntp - 1)
+    for u in range(groups):
+        row_start(REV + u, dstates[u, 0], decays[u])
+    loads[4].wait()
 
     def project(m, carry):
         x_load(m).wait()
@@ -483,15 +492,15 @@
         sig = sigmoid(pre)
         vals_s[rows, :] = pre * sig
         vslope_s[rows, :] = sig * (1.0 + pre * (1.0 - sig))
-        for i in range(per):
-            inner_grads(0, m * per + i)
+
+        inner_grads(0, lead + m)
         return carry
 
-    half = LOADS // 2
-    lax.fori_loop(0, half, project, 0)
-    for u in range(1, groups):
+    met = 3
+    lax.fori_loop(0, met, project, 0)
+    for u in range(groups):
         row_finish(REV + u, True)
-    lax.fori_loop(half, LOADS, project, 0)
+    lax.fori_loop(met, LOADS, project, 0)
     decayed = forward()
     for u in range(groups):
         row_start(FWD + u, states[u, blocks], decayed[:, lanes_of(u)])
@@ -514,11 +523,7 @@
         row_finish(FWD + u, False)
     chunks(0, Z, X * Z, quiet)
     for u in range(1, groups):
-        def inner(b, carry, u=u):
-            inner_grads(u, b)
-            return carry
-
-        lax.fori_loop(0, blocks, inner, 0, unroll=4)
+        lax.fori_loop(0, blocks, inner(u), 0, unroll=4)
         col_finish(REV + u, True, outgo_s, u)
         correct(u)
         chunks(u, 0, X * Z, early_step if u == 1 else quiet)
@@ -551,25 +556,32 @@
 
     lax.fori_loop(0, blocks // 2, both, 0)
     outs = [local(dkey_s, dkey_hbm, o_sem.at[0]), local(dquery_s, dquery_hbm, o_sem.at[1]),
-            local(dgate_s, dgate_hbm, o_sem.at[2])]
+            local(dgate_s, dgate_hbm, o_sem.at[2]), local(ddecay_s, ddecay_hbm, o_sem.at[4])]
     for copy in outs:
         copy.start()
-    if early + blocks < steps:
-        lax.fori_loop(early + blocks, steps, alone, 0)
-
-    own = X * Z - 1
-    for xi in range(X - 1):
-        xl_copy(xi).wait_recv()
-        part[own, 0:PIECE, :] += xlast[xi]
-    last = part[own]
-    norms[tpi] = jnp.broadcast_to(jnp.sum(last * last, axis=0, keepdims=True), (ROWS, CD))
-
     def norm_copy(d):
         return remote(norms.at[tpi], norms.at[tpi], ns.at[d - 1], nr.at[d - 1], "tp", lax.rem(tpi + d, ntp))
 
-    for d in range(1, ntp):
-        norm_copy(d).start()
-    wg_s[...] = last.T
+    own = X * Z - 1
+    squares = jnp.zeros((1, CD), F32)
+    seen = early + blocks
+    for u in range(groups):
+        until = pass0 + pass1 + (u + 1) * PU - 1
+        if seen < until:
+            lax.fori_loop(seen, until, alone, 0)
+            seen = until
+        if u == 0:
+            for xi in range(X - 1):
+                xl_copy(xi).wait_recv()
+                part[own, 0:PIECE, :] += xlast[xi]
+        rows = part[own, lanes_of(u), :]
+        squares = squares + jnp.sum(rows * rows, axis=0, keepdims=True)
+        if u == groups - 1:
+            norms[tpi] = jnp.broadcast_to(squares, (ROWS, CD))
+            for d in range(1, ntp):
+                norm_copy(d).start()
+        wg_s[:, lanes_of(u)] = rows.T
+
     wcopy = local(wg_s, wgrad_hbm, o_sem.at[3])
     wcopy.start()
 
@@ -606,10 +618,23 @@
     total = norms[0]
     for i in range(1, ntp):
         total = total + norms[i]
-    norm_ref[...] = total[0:1]
+    norm_s[...] = total[0:1]
+    ncopy = local(norm_s, norm_hbm, o_sem.at[5])
+    ncopy.start()
     for copy in outs:
         copy.wait()
     wcopy.wait()
+    ncopy.wait()
+
+
+def write(*refs):
+    count = len(refs) // 2
+    sem = refs[-1]
+    copies = [pltpu.make_async_copy(refs[i], refs[count + i], sem.at[i]) for i in range(count)]
+    for copy in copies:
+        copy.start()
+    for copy in copies:
+        copy.wait()
 
 
 def shards(block_input, value_weight, key_rows, query_rows, decay_pre, decay_log, gate_rows, out_grad):
@@ -635,14 +660,10 @@
     outs = pl.pallas_call(
         functools.partial(kernel, c),
         in_specs=[hbm, hbm, hbm, hbm, vmem, pl.BlockSpec(memory_space=pltpu.SMEM), hbm, hbm],
-        out_specs=[hbm, hbm, vmem, hbm, hbm, vmem],
+        out_specs=[hbm] * 6,
         out_shape=[
-            jax.ShapeDtypeStruct((tokens, narrow), F32),
-            jax.ShapeDtypeStruct((tokens, narrow), F32),
-            jax.ShapeDtypeStruct((heads, tokens), F32),
-            jax.ShapeDtypeStruct((tokens, wide), F32),
-            jax.ShapeDtypeStruct((cd, wide), F32),
-            jax.ShapeDtypeStruct((1, cd), F32),
+            V((tokens, narrow), F32), V((tokens, narrow), F32), V((heads, tokens), F32),
+            V((tokens, wide), F32), V((cd, wide), F32), V((1, cd), F32),
         ],
         scratch_shapes=[
             V((tokens, depth), BF), V((depth, wide), BF), V((tokens, narrow), BF), V((tokens, narrow), BF),
@@ -658,17 +679,26 @@
             V((2 * groups, X, STATE + ROWS, gw), F32), V((2 * groups, STATE + ROWS, gw), F32),
             V((2 * groups, Z - 1, STATE + ROWS, gw), F32),
             V((groups, STATE, gw), F32), V((groups, STATE, gw), F32), V((2 * groups, STATE + ROWS, gw), F32),
-            V((cd, wide), F32), V((ntp, ROWS, cd), F32),
+            V((cd, wide), F32), V((ntp, ROWS, cd), F32), V((heads, tokens), F32), V((1, cd), F32),
             dma((5,)), dma((LOADS,)),
             dma((2 * groups, XO)), dma((2 * groups, XO)), dma((2 * groups, Z - 1)), dma((2 * groups, Z - 1)),
             dma((XO * Z * NP,)), dma((XO * Z * NP,)), dma((Z * NP,)), dma(((Z + 1) * NP,)),
             dma((X * Z,)), dma((X * (Z + 1),)), dma((XO,)), dma((XO,)),
-            dma((ntp - 1,)), dma((ntp - 1,)), dma((4,)),
+            dma((ntp - 1,)), dma((ntp - 1,)), dma((6,)),
         ],
         compiler_params=pltpu.CompilerParams(
-            collective_id=0, has_side_effects=True, vmem_limit_bytes=66_000_000),
+            collective_id=0, has_side_effects=True, vmem_limit_bytes=60_000_000),
         name="mixer_back",
     )(block_input, value_weight, key_rows, query_rows, decay_pre, decay_log, gate_rows, out_grad)
+    outs = pl.pallas_call(
+        write,
+        in_specs=[vmem] * len(outs),
+        out_specs=[hbm] * len(outs),
+        out_shape=[jax.ShapeDtypeStruct(o.shape, o.dtype) for o in outs],
+        scratch_shapes=[dma((len(outs),))],
+        compiler_params=pltpu.CompilerParams(vmem_limit_bytes=1 << 20),
+        name="write_results",
+    )(*outs)
     key_grad, query_grad, decay_grad, gate_grad, weight_grad, norm = outs
     return key_grad, query_grad, decay_grad, gate_grad, weight_grad, norm.reshape(cd)
 

time: 77.5 us -> 70.7 us (0.912)
  local copies, waits for them, and re-layouts: 6.76 us -> 0 us
    unnamed x16 -> x0, local copies, waits for them, and re-layouts: 6.76 us -> none
    pallas_call x0 -> x1, Pallas kernels: none -> 2.24 us  [shards(): pl.pallas_call(write, in_specs=[vmem] * len(outs), out_specs=[hbm] * len(...]
    pallas_call x1, Pallas kernels: 69.8 us -> 67.6 us  [shards(): pl.pallas_call(functools.partial(kernel, c), in_specs=[hbm, hbm, hbm, hbm...]
where the time goes in v3:
time: 70.7 us; the launch traced here: 70.5 us
  Pallas kernels  69.9 us (99%)
    pallas_call x1, Pallas kernels, shards(): pl.pallas_call(functools.partial(kernel, c), in_specs=[hbm, hbm, hbm, hbm...  67.6 us
    pallas_call x1, Pallas kernels, shards(): pl.pallas_call(write, in_specs=[vmem] * len(outs), out_specs=[hbm] * len(...  2.24 us

profile of v3, /device:TPU:0, one launch (start us, length us, event | category | flops | bytes accessed | tf_op | source)
XLA Modules:
  0.0 70.5 jit_solution(15538551335009433843)
XLA Ops:
  0.6 67.6 %mixer_back.1 = (f32[2048,128]{1,0:T(8,128)S(1)}, f32[2048,128]{1,0:T(8,128)S(1)}, f32[4,2048]{1,0:T(4,128)S(1)}, f32[2048,256]{1,0:T(8,128)S(1)}, f32[512,256]{1,0:T(8,128)S(1)}, /*index=5*/f32[1,512]{1,0:T(1,128)S(1)}) custom-call(bf16[2048,4096]{1,0:T(8,128)(2,1)} %x_hbm.1, bf16[4096,256]{1,0:T(8,128)(2,1)} %w_hbm.1, bf16[2048,128]{1,0:T(8,128)(2,1)} %key_hbm.1, ...), custom_call_target="tpu_custom_call" | custom-call | tf_op jit(solution)/shard_map/mixer_back/pallas_call | solution.py:660
  68.3 2.2 %write_results.1 = (f32[2048,128]{1,0:T(8,128)}, f32[2048,128]{1,0:T(8,128)}, f32[4,2048]{1,0:T(4,128)}, f32[2048,256]{1,0:T(8,128)}, f32[512,256]{1,0:T(8,128)}, /*index=5*/f32[1,512]{1,0:T(1,128)}) custom-call(f32[2048,128]{1,0:T(8,128)S(1)} %get-tuple-element.18.refs_0_, f32[2048,128]{1,0:T(8,128)S(1)} %get-tuple-element.19.refs_1_, ...), custom_call_target="tpu_custom_call" | custom-call | tf_op jit(solution)/shard_map/write_results/pallas_call | solution.py:693

commit v4 on v3

--- a/solution.py
+++ b/solution.py
@@ -11,7 +11,7 @@
 STATE = 64
 BLK = 128
 ROWS = 8
-LOADS = 8
+LOADS = 4
 PIECE = 32
 
 BF = jnp.bfloat16
@@ -76,7 +76,7 @@
     loads = [local(gate_hbm, gv, in_sem.at[0]), local(out_hbm, ov, in_sem.at[1]),
              local(query_hbm, qv, in_sem.at[2]), local(key_hbm, kv, in_sem.at[3]),
              local(w_hbm, wv, in_sem.at[4])]
-    for copy in loads[:3]:
+    for copy in loads:
         copy.start()
     XR = tokens // LOADS
 
@@ -190,8 +190,8 @@
 
     for copy in loads[:3]:
         copy.wait()
-    for copy in loads[3:]:
-        copy.start()
+    for m in range(LOADS):
+        x_load(m).start()
 
     def reverse(u):
         gs = lanes_of(u)
@@ -223,12 +223,7 @@
         tk = toks(b)
         run = run_s[heads8(b), :]
         key, query = kv[tk, :], qv[tk, :]
-        if u == 0:
-            te_all = to_end(b)
-            te_s[tk, :] = te_all
-            te = te_all[:, gs]
-        else:
-            te = te_s[tk, gs]
+        te = te_s[tk, gs]
         mine = iota((BLK, narrow), 1) // STATE == u
         scores = dot(key, jnp.where(mine, query, jnp.zeros_like(query)), 1, 1)
         cols = cols_s[tk, :]
@@ -464,26 +459,18 @@
             z_copy(k, q).start()
 
     REV, FWD = 0, groups
-    decays = []
+    decays = [reverse(u) for u in range(groups)]
+    pl.semaphore_wait(barrier, n - 1 + ntp - 1)
     for u in range(groups):
-        decays.append(reverse(u))
-        if u == 0:
-            for m in range(LOADS):
-                x_load(m).start()
-    loads[3].wait()
+        row_start(REV + u, dstates[u, 0], decays[u])
+    for copy in loads[3:]:
+        copy.wait()
 
     def inner(u):
         def body(b, carry):
             inner_grads(u, b)
             return carry
         return body
-
-    lead = max(0, blocks - LOADS)
-    lax.fori_loop(0, lead, inner(0), 0, unroll=4)
-    pl.semaphore_wait(barrier, n - 1 + ntp - 1)
-    for u in range(groups):
-        row_start(REV + u, dstates[u, 0], decays[u])
-    loads[4].wait()
 
     def project(m, carry):
         x_load(m).wait()
@@ -492,11 +479,15 @@
         sig = sigmoid(pre)
         vals_s[rows, :] = pre * sig
         vslope_s[rows, :] = sig * (1.0 + pre * (1.0 - sig))
-
-        inner_grads(0, lead + m)
+        for i in range(blocks // LOADS):
+            b = m * (blocks // LOADS) + i
+            te_s[toks(b), :] = to_end(b)
+            if i < beside:
+                inner_grads(0, b)
         return carry
 
-    met = 3
+    beside = min(2, blocks // LOADS)
+    met = LOADS // 2
     lax.fori_loop(0, met, project, 0)
     for u in range(groups):
         row_finish(REV + u, True)
@@ -504,6 +495,14 @@
     decayed = forward()
     for u in range(groups):
         row_start(FWD + u, states[u, blocks], decayed[:, lanes_of(u)])
+
+    def others(m, carry):
+        for i in range(beside, blocks // LOADS):
+            inner_grads(0, m * (blocks // LOADS) + i)
+        return carry
+
+    if beside < blocks // LOADS:
+        lax.fori_loop(0, LOADS, others, 0, unroll=2)
     col_finish(REV, True, outgo_s, 0)
     correct(0)
     steps = Z * (NP - 1)

time: 70.7 us -> 69.5 us (0.983)
  Pallas kernels: 69.9 us -> 68.6 us
    pallas_call x1, Pallas kernels: 67.6 us -> 66.4 us  [shards(): pl.pallas_call(functools.partial(kernel, c), in_specs=[hbm, hbm, hbm, hbm...]
where the time goes in v4:
time: 69.5 us; the launch traced here: 69.3 us
  Pallas kernels  68.6 us (99%)
    pallas_call x1, Pallas kernels, shards(): pl.pallas_call(functools.partial(kernel, c), in_specs=[hbm, hbm, hbm, hbm...  66.4 us
    pallas_call x1, Pallas kernels, shards(): pl.pallas_call(write, in_specs=[vmem] * len(outs), out_specs=[hbm] * len(...  2.24 us

profile of v4, /device:TPU:0, one launch (start us, length us, event | category | flops | bytes accessed | tf_op | source)
XLA Modules:
  0.0 69.3 jit_solution(15431587472896933706)
XLA Ops:
  0.6 66.4 %mixer_back.1 = (f32[2048,128]{1,0:T(8,128)S(1)}, f32[2048,128]{1,0:T(8,128)S(1)}, f32[4,2048]{1,0:T(4,128)S(1)}, f32[2048,256]{1,0:T(8,128)S(1)}, f32[512,256]{1,0:T(8,128)S(1)}, /*index=5*/f32[1,512]{1,0:T(1,128)S(1)}) custom-call(bf16[2048,4096]{1,0:T(8,128)(2,1)} %x_hbm.1, bf16[4096,256]{1,0:T(8,128)(2,1)} %w_hbm.1, bf16[2048,128]{1,0:T(8,128)(2,1)} %key_hbm.1, ...), custom_call_target="tpu_custom_call" | custom-call | tf_op jit(solution)/shard_map/mixer_back/pallas_call | solution.py:659
  67.0 2.2 %write_results.1 = (f32[2048,128]{1,0:T(8,128)}, f32[2048,128]{1,0:T(8,128)}, f32[4,2048]{1,0:T(4,128)}, f32[2048,256]{1,0:T(8,128)}, f32[512,256]{1,0:T(8,128)}, /*index=5*/f32[1,512]{1,0:T(1,128)}) custom-call(f32[2048,128]{1,0:T(8,128)S(1)} %get-tuple-element.18.refs_0_, f32[2048,128]{1,0:T(8,128)S(1)} %get-tuple-element.19.refs_1_, ...), custom_call_target="tpu_custom_call" | custom-call | tf_op jit(solution)/shard_map/write_results/pallas_call | solution.py:692

commit v5 on v4

--- a/solution.py
+++ b/solution.py
@@ -216,7 +216,7 @@
             dstates[u, b] = dstates[u, b + 1] * factor + back
             return decayed * factor
 
-        return lax.fori_loop(0, blocks, body, jnp.ones((ROWS, gw), F32), unroll=4)
+        return lax.fori_loop(0, blocks, body, jnp.ones((ROWS, gw), F32), unroll=8)
 
     def inner_grads(u, b):
         gs = lanes_of(u)
@@ -264,7 +264,7 @@
             vgt_s[gs, tk] = (dval * vslope_s[tk, gs]).T.astype(BF)
             return carry
 
-        lax.fori_loop(0, blocks, body, 0, unroll=4)
+        lax.fori_loop(0, blocks, body, 0, unroll=8)
 
     def chunk_of(k):
         out = jnp.int32(0)
@@ -502,7 +502,7 @@
         return carry
 
     if beside < blocks // LOADS:
-        lax.fori_loop(0, LOADS, others, 0, unroll=2)
+        lax.fori_loop(0, LOADS, others, 0, unroll=4)
     col_finish(REV, True, outgo_s, 0)
     correct(0)
     steps = Z * (NP - 1)

time: 69.5 us -> 68.3 us (0.983)
  Pallas kernels: 68.6 us -> 67.4 us
    pallas_call x1, Pallas kernels: 66.4 us -> 65.2 us  [shards(): pl.pallas_call(functools.partial(kernel, c), in_specs=[hbm, hbm, hbm, hbm...]
where the time goes in v5:
time: 68.3 us; the launch traced here: 68.1 us
  Pallas kernels  67.4 us (99%)
    pallas_call x1, Pallas kernels, shards(): pl.pallas_call(functools.partial(kernel, c), in_specs=[hbm, hbm, hbm, hbm...  65.2 us
    pallas_call x1, Pallas kernels, shards(): pl.pallas_call(write, in_specs=[vmem] * len(outs), out_specs=[hbm] * len(...  2.24 us

profile of v5, /device:TPU:0, one launch (start us, length us, event | category | flops | bytes accessed | tf_op | source)
XLA Modules:
  0.0 68.1 jit_solution(14168653800771946219)
XLA Ops:
  0.6 65.2 %mixer_back.1 = (f32[2048,128]{1,0:T(8,128)S(1)}, f32[2048,128]{1,0:T(8,128)S(1)}, f32[4,2048]{1,0:T(4,128)S(1)}, f32[2048,256]{1,0:T(8,128)S(1)}, f32[512,256]{1,0:T(8,128)S(1)}, /*index=5*/f32[1,512]{1,0:T(1,128)S(1)}) custom-call(bf16[2048,4096]{1,0:T(8,128)(2,1)} %x_hbm.1, bf16[4096,256]{1,0:T(8,128)(2,1)} %w_hbm.1, bf16[2048,128]{1,0:T(8,128)(2,1)} %key_hbm.1, ...), custom_call_target="tpu_custom_call" | custom-call | tf_op jit(solution)/shard_map/mixer_back/pallas_call | solution.py:659
  65.8 2.2 %write_results.1 = (f32[2048,128]{1,0:T(8,128)}, f32[2048,128]{1,0:T(8,128)}, f32[4,2048]{1,0:T(4,128)}, f32[2048,256]{1,0:T(8,128)}, f32[512,256]{1,0:T(8,128)}, /*index=5*/f32[1,512]{1,0:T(1,128)}) custom-call(f32[2048,128]{1,0:T(8,128)S(1)} %get-tuple-element.18.refs_0_, f32[2048,128]{1,0:T(8,128)S(1)} %get-tuple-element.19.refs_1_, ...), custom_call_target="tpu_custom_call" | custom-call | tf_op jit(solution)/shard_map/write_results/pallas_call | solution.py:692
